TPU v7x, 512 devices: a 4x2x32 block of a 4x8x32 slice. The times are simulated.
512 devices in a mesh: grp: 2 (over y), sp: 32 (over z), dp: 8 (over x, core).
Axes of the slice: x: 4, y: 2, z: 32, core: 2. Of those that a mesh axis runs over, the one named last changes fastest.
The devices are a block of a 4x8x32 slice.
Arguments:
- tokens: bfloat16 [16, 12288, 2048], P(('grp', 'dp'), 'sp'), parts along dimension 0, may hold values from -6 to 6
- w_value: bfloat16 [2048, 1024], P('dp', 'sp'), may hold values from -0.125 to 0.125
- w_gate: bfloat16 [2048, 1024], P('dp', 'sp'), may hold values from -0.125 to 0.125
- conv_weight: bfloat16 [31, 1024], replicated, may hold values from -20 to 20
- norm_gain: float32 [1024], replicated, may hold values from 0.1 to 1.9
- norm_bias: float32 [1024], replicated, may hold values from -3 to 3
- w_out: bfloat16 [1024, 2048], P('sp', 'dp'), may hold values from -0.1875 to 0.1875
Outputs:
- mixed: bfloat16 [16, 12288, 2048], P(('grp', 'dp'), 'sp'), parts along dimension 0
There are 2 independent parts, one for each index of `grp`. A program takes and returns all parts, laid end to end along the dimension named above; an argument that names none is the same for every part. Nothing has to cross between parts.
All inputs are finite; a program needn't handle non-finite values.
Results may differ from a plain program's by a relative error of at most 0.012.
Values may be sent and summed in bfloat16 or wider, within the bound.
No kernel may reach another device: no remote copies, remote signals or barrier semaphores. Data moves between devices by JAX's collectives and lax.ppermute only.
A program may use at most 64 MiB of HBM per device.

v0:
```python
import jax
import jax.numpy as jnp
from jax import lax
from jax.sharding import PartitionSpec as P

EPS = 1e-05


def rows_first(arrays, axis, dims):
    turned = [jnp.moveaxis(a, dim, 0) for a, dim in zip(arrays, dims)]
    both = jnp.concatenate([t.reshape(len(t), -1) for t in turned], axis=1)
    out, at, finished = (lax.all_gather(both, axis, axis=0, tiled=True), 0, [])
    for t, dim in zip(turned, dims):
        share = out[:, at : at + t[0].size].reshape(-1, *t.shape[1:])
        finished.append(jnp.moveaxis(share, 0, dim))
        at += t[0].size
    return tuple(finished)


def passed_along(array, axis, by):
    peers = lax.axis_size(axis)
    pairs = [(i, i + by) for i in range(peers) if 0 <= i + by < peers]
    return lax.ppermute(array, axis, pairs)


def per_device(tokens, w_value, w_gate, conv_weight, norm_gain, norm_bias, w_out):
    pieces = rows_first((w_value, w_gate, w_out), "dp", (0, 0, 1))
    full_value, full_gate, full_out = rows_first((pieces[0], pieces[1], pieces[2]), "sp", (1, 1, 0))
    rows = tokens[0]
    kernel_width = conv_weight.shape[0]
    channels = norm_gain.shape[0]
    value = jnp.dot(rows, full_value, preferred_element_type=jnp.float32)
    gate = jnp.dot(rows, full_gate, preferred_element_type=jnp.float32)
    glu = (value * jax.nn.sigmoid(gate)).astype(jnp.bfloat16)
    earlier = passed_along(glu[rows.shape[0] - (kernel_width - 1) :], "sp", 1)
    extended = jnp.concatenate([earlier, glu], axis=0)
    kernel = conv_weight[::-1][:, None, :]
    conv = lax.conv_general_dilated(
        extended[None],
        kernel,
        (1,),
        [(0, 0)],
        dimension_numbers=("NWC", "WIO", "NWC"),
        feature_group_count=channels,
        preferred_element_type=jnp.float32,
    )[0].astype(jnp.bfloat16)
    conv_f = conv.astype(jnp.float32)
    mean = jnp.mean(conv_f, axis=1, keepdims=True)
    meansq = jnp.mean(conv_f * conv_f, axis=1, keepdims=True)
    scaled = (conv_f - mean) * lax.rsqrt(meansq - mean * mean + EPS) * norm_gain + norm_bias
    normed = jax.nn.silu(scaled).astype(jnp.bfloat16)
    mixed = jnp.dot(normed, full_out, preferred_element_type=jnp.float32)
    return mixed.astype(jnp.bfloat16)[None]


def solution(mesh):
    placed = (
        P(("grp", "dp"), "sp", None),
        P("dp", "sp"),
        P("dp", "sp"),
        P(),
        P(),
        P(),
        P("sp", "dp"),
    )
    return jax.shard_map(
        per_device,
        mesh=mesh,
        in_specs=placed,
        out_specs=P(("grp", "dp"), "sp", None),
        check_vma=False,
    )
```

profile of v0, /device:TPU:34, one launch (start us, length us, event | category | flops | bytes accessed | tf_op | source)
XLA Modules:
  0.0 246.4 jit_solution(5164028319720590578)
XLA Ops:
  6.6 0.9 pad_maximum_fusion.1
  7.4 50.4 %all_gather.6 = bf16[2048,96]{0,1:T(8,128)(2,1)S(1)} all-gather(bf16[256,96]{0,1:T(8,128)(2,1)S(1)} %pad_maximum_fusion.1), channel_id=1, replica_groups=mesh['grp'=2,'sp'=32,'dp'=8] {'dp'}, dimensions={0}, use_global_device_ids=true | all-gather | bytes 442368 | tf_op jit(solution)/shard_map/all_gather | solution.py:12
  57.9 0.8 pad_maximum_fusion
  58.7 0.1 all-gather.2.cloned.1.call-update
  58.7 153.0 %all-gather.2.cloned.1.call-done = bf16[1024,6144]{1,0:T(8,128)(2,1)} async-done(((bf16[32,6144]{1,0:T(8,128)(2,1)}), bf16[1024,6144]{1,0:T(8,128)(2,1)}) %all-gather.2.cloned.1.call-update) | async-done | bytes 12582928 | tf_op jit(solution)/shard_map/all_gather | solution.py:12
  211.7 4.0 %fusion.2 = f32[1024,384]{0,1:T(8,128)S(1)} fusion(bf16[1024,6144]{1,0:T(8,128)(2,1)} %all-gather.2.cloned.1.call-done, bf16[1,384,2048]{2,1,0:T(8,128)(2,1)S(1)} %copy-done), kind=kOutput, calls=%fused_computation.2 | convolution fusion | flops 1610612736 | bytes 7340032 | tf_op jit(solution)/shard_map/dot_general | solution.py:33
  215.8 4.1 %fusion.30 = bf16[384,1024]{1,0:T(8,128)(2,1)S(1)} fusion(f32[1024,384]{0,1:T(8,128)S(1)} %fusion.2, bf16[1,384,2048]{2,1,0:T(8,128)(2,1)S(1)} %copy-done, bf16[1024,6144]{1,0:T(8,128)(2,1)} %all-gather.2.cloned.1.call-done), kind=kOutput, calls=%fused_computation.28 | convolution fusion | flops 1612578816 | bytes 8126464 | tf_op jit(solution)/shard_map/dot_general | solution.py:32
  219.9 3.0 %collective-permute-start = (bf16[30,1024]{1,0:T(8,128)(2,1)S(1)}, bf16[30,1024]{1,0:T(8,128)(2,1)S(1)}, u32[]{:S(2)}, u32[]{:S(2)}) collective-permute-start(bf16[30,1024]{1,0:T(8,128)(2,1)S(1)} %slice.35), channel_id=1, source_target_pairs={{0,8},{8,16},{16,24},{24,32},{32,40},{40,48},{48,56},{56,64},{64,7... | collective-permute-start | bytes 184328 | tf_op jit(solution)/shard_map/ppermute | solution.py:23
  222.9 0.3 rev.3
  223.2 1.4 collective-permute-done
  224.6 0.2 maximum_bitcast_fusion
  224.8 0.1 pad
  224.9 0.2 reshape.24
  225.1 0.5 copy.12
  225.5 0.1 slice.36
  225.7 0.1 copy-done.4
  225.7 3.8 %fusion.37 = f32[8,52,1024]{2,0,1:T(8,128)S(1)} fusion(bf16[1,7,30,1024]{3,1,2,0:T(8,128)(2,1)S(1)} %slice.36, bf16[1,8,52,1024]{3,1,2,0:T(8,128)(2,1)S(1)} %copy.12, pred[8,52]{0,1:T(8,128)(4,1)S(1)} %copy-done.4, bf16[31,1,1024]{2,0,1:T(8,128)(2,1)S(1)} %bitcast.44), kind=kOutput, calls=%fused_computation.29 | convolution fusion | flops 31719424 | bytes 3049888 | tf_op jit(solution)/shard_map/conv_general_dilated | solution.py:38
  229.5 2.3 copy.14
  231.8 1.6 reshape.28
  233.4 0.2 fusion.16
  233.6 0.2 slice_reduce_fusion
  233.7 0.3 copy-done.2
  234.0 0.0 copy-done.3
  234.1 5.5 %fusion.10 = bf16[1,384,2048]{2,1,0:T(8,128)(2,1)} fusion(bf16[1024,6144]{1,0:T(8,128)(2,1)} %all-gather.2.cloned.1.call-done, f32[1,416,1024]{2,1,0:T(8,128)S(1)} %reshape.28, f32[1024]{0:T(1024)S(1)} %copy-done.2, f32[1024]{0:T(1024)S(1)} %copy-done.3, f32[384]{0:T(512)S(1)} %get-tuple-element.9, f32[384]{0:T(512)S(1)} %get-tuple-element.8), kind=kOutput, calls=%fused_computation.9 | convolution fusion | flops 1614938112 | bytes 7352320 | tf_op jit(solution)/shard_map/dot_general | solution.py:52
  (11 shorter events, 0.1 us)
Async XLA Ops:
  6.5 205.2 %copy-start = (bf16[1,384,2048]{2,1,0:T(8,128)(2,1)S(1)}, bf16[1,384,2048]{2,1,0:T(8,128)(2,1)}, u32[]{:S(2)}) copy-start(bf16[1,384,2048]{2,1,0:T(8,128)(2,1)} %param.7) | copy-start | bytes 4718596
  6.6 205.2 %all-gather.2.cloned.1.call-start = ((), (), s32[]{:S(2)}) async-start(), calls=%async_computation | async-start | bytes 12976128 | tf_op jit(solution)/shard_map/all_gather | solution.py:12
  215.7 7.2 %copy-start.1 = (bf16[31,1024]{1,0:T(8,128)(2,1)S(1)}, bf16[31,1024]{1,0:T(8,128)(2,1)}, u32[]{:S(2)}) copy-start(bf16[31,1024]{1,0:T(8,128)(2,1)} %param.10) | copy-start | bytes 190468
  219.9 4.7 %collective-permute-start = (bf16[30,1024]{1,0:T(8,128)(2,1)S(1)}, bf16[30,1024]{1,0:T(8,128)(2,1)S(1)}, u32[]{:S(2)}, u32[]{:S(2)}) collective-permute-start(bf16[30,1024]{1,0:T(8,128)(2,1)S(1)} %slice.35), channel_id=1, source_target_pairs={{0,8},{8,16},{16,24},{24,32},{32,40},{40,48},{48,56},{56,64},{64,7... | collective-permute-start | bytes 184328 | tf_op jit(solution)/shard_map/ppermute | solution.py:23
  225.0 0.7 copy-start.4
  233.4 0.7 copy-start.2
  233.4 0.7 copy-start.3
Sparse Core Ops, SparseCore 0:
  58.9 152.8 all-gather.1
where the time goes:
time: 247 us; the launch traced here: 246 us
  waiting for transfers between devices  154 us (62%)
  blocking collectives  50.4 us (20%)
  matrix products  17.4 us (7%)
  between operations  13.6 us (6%)
  local copies, waits for them, and re-layouts  5.38 us (2%)
  starting transfers between devices  2.97 us (1%)
    all_gather x1, waiting for transfers between devices, rows_first(): out, at, finished = (lax.all_gather(both, axis, axis=0, tiled=True), 0, [])  153 us
    all_gather x1, blocking collectives, rows_first(): out, at, finished = (lax.all_gather(both, axis, axis=0, tiled=True), 0, [])  50.4 us
    dot_general x1, matrix products, per_device(): mixed = jnp.dot(normed, full_out, preferred_element_type=jnp.float32)  5.51 us
  transfers between devices with their start and end apart: 2, of which 2 were waited for; matrix products, arithmetic and copies ran while one was open for 0% of the time, Pallas kernels for 0%

commit v1 on v0

v1 whole, which is shorter than its diff:
```python
import jax
import jax.numpy as jnp
from jax import lax
from jax.experimental import pallas as pl
from jax.experimental.pallas import tpu as pltpu
from jax.sharding import Mesh, PartitionSpec as P


EPS = 1e-05
HALO = 32
PIECE = 256
LANES = 128


def spread(block, axis):
    members = lax.axis_size(axis)
    return lax.all_to_all(jnp.broadcast_to(block, (members, *block.shape)), axis, 0, 0)


def swapped(array, axis):
    return lax.ppermute(array, axis, [(0, 1), (1, 0)])


def columns(where_ref, x, m, deep):
    core = where_ref[0]
    c = core if m == 0 else 1 - core
    return pl.ds(pl.multiple_of((2 * x + c) * deep, deep), deep)


def convolve(where_ref, halo_ref, tok_ref, cw_ref, vg0_ref, vg1_ref, conv_ref, stats_ref, tok, shifted):
    par = where_ref[1]
    rows, part = conv_ref.shape
    taps = cw_ref.shape[1]
    blocks, deep = vg0_ref.shape[0], vg0_ref.shape[-1]
    order = [(x, m) for x in range(blocks) for m in range(2)]
    for at, (x, m) in enumerate(order):
        here = slice(at * deep, (at + 1) * deep)
        tok[:HALO, here] = halo_ref[:, columns(where_ref, x, m, deep)]
        tok[HALO:, here] = tok_ref[:, columns(where_ref, x, m, deep)]

    half = rows // 2
    for q in range(part // PIECE):
        span = slice(q * PIECE, (q + 1) * PIECE)

        def product(m):
            piece = jnp.concatenate([(vg0_ref, vg1_ref)[c][x, m, span, :] for x, c in order], axis=1)
            return lax.dot_general(tok[...], piece, (((1,), (1,)), ((), ())), preferred_element_type=jnp.float32)

        value, gate = product(0), product(1)
        glu = (value * jax.nn.sigmoid(gate)).astype(jnp.bfloat16).astype(jnp.float32)
        shifted[0] = glu
        for r in range(1, 8):
            shifted[r] = pltpu.roll(glu, r, 0)
        for l in range(PIECE // LANES):
            lanes = slice(l * LANES, (l + 1) * LANES)
            at = q * PIECE + l * LANES
            for h in range(2):
                acc = jnp.zeros((half, LANES), jnp.float32)
                for k in range(taps):
                    r, j = k % 8, k // 8
                    begin = HALO - 8 * j + h * half
                    acc = acc + cw_ref[par, k : k + 1, at : at + LANES] * shifted[r, begin : begin + half, lanes]
                acc = acc.astype(jnp.bfloat16)
                when = slice(h * half, (h + 1) * half)
                conv_ref[when, at : at + LANES] = acc
                acc = acc.astype(jnp.float32)
                if q == 0 and l == 0:
                    stats_ref[0, when] = acc
                    stats_ref[1, when] = acc * acc
                else:
                    stats_ref[0, when] += acc
                    stats_ref[1, when] += acc * acc


def finish(where_ref, conv_a_ref, conv_b_ref, stats_a_ref, stats_b_ref, gain_ref, bias_ref, o0_ref, o1_ref, out_ref, normed):
    side = where_ref[1]
    part = conv_a_ref.shape[1]
    blocks, deep = o0_ref.shape[1], o0_ref.shape[-1]
    mean = jnp.sum(stats_a_ref[0] + stats_b_ref[0], axis=1, keepdims=True) / (2 * part)
    meansq = jnp.sum(stats_a_ref[1] + stats_b_ref[1], axis=1, keepdims=True) / (2 * part)
    scale = lax.rsqrt(meansq - mean * mean + EPS)
    for s, conv_ref in enumerate((conv_a_ref, conv_b_ref)):
        par = side if s == 0 else 1 - side
        for q in range(part // PIECE):
            span = slice(q * PIECE, (q + 1) * PIECE)
            v = (conv_ref[:, span].astype(jnp.float32) - mean) * scale * gain_ref[par, :, span] + bias_ref[par, :, span]
            here = slice(s * part + q * PIECE, s * part + (q + 1) * PIECE)
            normed[:, here] = (v / (1.0 + jnp.exp(-v))).astype(jnp.bfloat16)
    for x in range(blocks):
        for m, o_ref in enumerate((o0_ref, o1_ref)):
            right = jnp.concatenate([o_ref[0, x], o_ref[1, x]], axis=0)
            out = jnp.dot(normed[...], right, preferred_element_type=jnp.float32)
            out_ref[:, columns(where_ref, x, m, deep)] = out.astype(jnp.bfloat16)


SMEM, VMEM = (pl.BlockSpec(memory_space=space) for space in (pltpu.SMEM, pltpu.VMEM))


def kernel(function, out_shape, scratch, flops, mib, *operands):
    single = not isinstance(out_shape, tuple)
    return pl.pallas_call(
        function,
        out_shape=out_shape,
        in_specs=[SMEM] + [VMEM] * (len(operands) - 1),
        out_specs=VMEM if single else (VMEM,) * len(out_shape),
        scratch_shapes=scratch,
        compiler_params=pltpu.CompilerParams(vmem_limit_bytes=mib * 1024 * 1024),
        cost_estimate=pl.CostEstimate(flops=flops, bytes_accessed=8 * 1024 * 1024, transcendentals=0),
    )(*operands)


def by_side(array, positions):
    k = array.shape[0]
    return array.reshape(k, positions, 2, -1).transpose(2, 0, 1, 3).reshape(2, k, -1)


def per_device(tokens, w_value, w_gate, conv_weight, norm_gain, norm_bias, w_out):
    rows = tokens[0]
    length, depth = rows.shape
    channels = conv_weight.shape[1]
    positions = lax.axis_size(("zh", "zl"))
    core, side = lax.axis_index("core"), lax.axis_index("side")
    both = jnp.stack([w_value.T, w_gate.T, w_out])
    half = both.shape[1] // 2
    mine = lax.dynamic_slice_in_dim(both, side * half, half, 1)
    far = lax.all_gather(mine, "zh", axis=0, tiled=True)
    near = lax.all_gather(far, "zl", axis=0, tiled=True)
    near = near.reshape(lax.axis_size("zl"), lax.axis_size("zh"), *mine.shape)
    near = near.transpose(2, 1, 0, 3, 4).reshape(3, positions * half, -1)
    last = rows[length - HALO :]
    near, last, conv_weight, norm_gain, norm_bias = lax.optimization_barrier((near, last, conv_weight, norm_gain, norm_bias))
    vg, o = near[:2], near[2]
    vg_other = swapped(vg, "side")
    halo = lax.ppermute(last, ("zh", "zl"), [(i, i + 1) for i in range(positions - 1)])
    oa = spread(o, "x")
    ob = swapped(oa, "side")
    vga0 = spread(vg, "x")
    vga1 = swapped(vga0, "core")
    vgb0 = spread(vg_other, "x")
    vgb1 = swapped(vgb0, "core")
    o0 = jnp.stack([oa, ob])
    o1 = swapped(o0, "core")
    taps = by_side(conv_weight.astype(jnp.float32), positions)
    gain, bias = by_side(norm_gain[None], positions), by_side(norm_bias[None], positions)
    here, there = (jnp.stack([core, s]).astype(jnp.int32) for s in (side, 1 - side))
    part = channels // 2
    made = (jax.ShapeDtypeStruct((length, part), jnp.bfloat16), jax.ShapeDtypeStruct((2, length, LANES), jnp.float32))
    scratch = [
        pltpu.VMEM((length + HALO, depth), jnp.bfloat16),
        pltpu.VMEM((8, length + HALO, PIECE), jnp.float32),
    ]
    flops = 2 * length * depth * channels
    conv_a, stats_a = kernel(convolve, made, scratch, flops, 20, here, halo, rows, taps, vga0, vga1)
    conv_b, stats_b = kernel(convolve, made, scratch, flops, 20, there, halo, rows, taps, vgb0, vgb1)
    mixed = kernel(
        finish, jax.ShapeDtypeStruct((length, depth), jnp.bfloat16),
        [pltpu.VMEM((length, channels), jnp.bfloat16)], flops, 16,
        here, conv_a, conv_b, stats_a, stats_b, gain, bias, o0, o1,
    )
    return mixed[None]


def solution(mesh):
    groups, positions, columns = (mesh.shape[a] for a in ("grp", "sp", "dp"))
    fine = Mesh(
        mesh.devices.reshape(groups // 2, 2, positions // 2, 2, columns // 2, 2),
        ("pair", "side", "zh", "zl", "x", "core"),
    )
    z, dp = ("zh", "zl"), ("x", "core")
    placed = (
        P(("pair", "side", *dp), z, None),
        P(dp, z),
        P(dp, z),
        P(),
        P(),
        P(),
        P(z, dp),
    )
    return jax.shard_map(
        per_device,
        mesh=fine,
        in_specs=placed,
        out_specs=P(("pair", "side", *dp), z, None),
        check_vma=False,
    )
```

time: 247 us -> 182 us (0.74)
  the two profiles are of different devices: /device:TPU:34 before, /device:TPU:33 now
where the time goes in v1:
time: 182 us
  blocking collectives  76.7 us (42%)
  starting transfers between devices  51.5 us (28%)
  waiting for transfers between devices  22.4 us (12%)
  Pallas kernels  17.9 us (10%)
  local copies, waits for them, and re-layouts  9.15 us (5%)
  other arithmetic  3.66 us (2%)
    all_gather x1, blocking collectives, per_device(): far = lax.all_gather(mine, 'zh', axis=0, tiled=True)  69 us
    ppermute x5, starting transfers between devices, swapped(): return lax.ppermute(array, axis, [(0, 1), (1, 0)])  35.4 us
    pallas_call x3, Pallas kernels, kernel(): pl.pallas_call(function, out_shape=out_shape, in_specs=[SMEM] + [VMEM] *...  17.9 us
    all_to_all x3, waiting for transfers between devices, spread(): lax.all_to_all(jnp.broadcast_to(block, (members, *block.shape)), axis, 0, 0)  15.2 us
    all_to_all x3, starting transfers between devices, spread(): lax.all_to_all(jnp.broadcast_to(block, (members, *block.shape)), axis, 0, 0)  12.4 us
    all_gather x1, blocking collectives, per_device(): near = lax.all_gather(far, 'zl', axis=0, tiled=True)  7.68 us
    ppermute x5, waiting for transfers between devices, swapped(): return lax.ppermute(array, axis, [(0, 1), (1, 0)])  6.88 us
    broadcast_in_dim x3, local copies, waits for them, and re-layouts, spread(): jnp.broadcast_to(block, (members, *block.shape))  5.05 us
  transfers between devices with their start and end apart: 9, of which 4 were waited for; matrix products, arithmetic and copies ran while one was open for 3% of the time, Pallas kernels for 7%

profile of v1, /device:TPU:33, one launch (start us, length us, event | category | flops | bytes accessed | tf_op | source)
XLA Modules:
  0.0 181.5 jit_solution(5938898293088683504)
XLA Ops:
  0.7 69.0 %all_gather.6 = bf16[48,16,256]{2,1,0:T(8,128)(2,1)S(1)} all-gather(bf16[3,16,256]{2,1,0:T(8,128)(2,1)S(1)} %fusion.1), channel_id=1, replica_groups=mesh['pair'=1,'side'=2,'zh'=16,'zl'=2,'x'=4,'core'=2] {'zh'}, dimensions={0}, use_global_device_ids=true | all-gather | bytes 417792 | tf_op jit(solution)/shard_map/all_gather | solution.py:126
  69.8 7.7 %all_gather.7 = bf16[96,16,256]{2,1,0:T(8,128)(2,1)S(1)} all-gather(bf16[48,16,256]{2,1,0:T(8,128)(2,1)S(1)} %all_gather.6), channel_id=1, replica_groups=mesh['pair'=1,'side'=2,'zh'=16,'zl'=2,'x'=4,'core'=2] {'zl'}, dimensions={0}, use_global_device_ids=true | all-gather | bytes 1179648 | tf_op jit(solution)/shard_map/all_gather | solution.py:127
  77.6 0.9 slice_bitcast_fusion.1
  78.5 1.0 broadcast_in_dim.14
  79.6 4.1 %all-to-all-start.2 = ((bf16[4,512,256]{2,1,0:T(8,128)(2,1)}), bf16[4,512,256]{2,1,0:T(8,128)(2,1)S(1)}, u32[]{:S(2)}, u32[]{:S(2)}) async-start(bf16[4,512,256]{2,1,0:T(8,128)(2,1)} %broadcast_in_dim.14), calls=%async_computation.2 | async-start | bytes 2097152 | tf_op jit(solution)/shard_map/all_to_all | solution.py:17
  83.8 9.7 %all-to-all-done.2 = bf16[4,512,256]{2,1,0:T(8,128)(2,1)S(1)} async-done(((bf16[4,512,256]{2,1,0:T(8,128)(2,1)}), bf16[4,512,256]{2,1,0:T(8,128)(2,1)S(1)}, u32[]{:S(2)}, u32[]{:S(2)}) %all-to-all-start.2) | async-done | bytes 1048608 | tf_op jit(solution)/shard_map/all_to_all | solution.py:17
  93.4 1.5 broadcast_in_dim.12
  94.9 3.7 %all-to-all-start = ((bf16[4,2,512,256]{3,2,1,0:T(8,128)(2,1)}), bf16[4,2,512,256]{3,2,1,0:T(8,128)(2,1)S(1)}, u32[]{:S(2)}, u32[]{:S(2)}) async-start(bf16[4,2,512,256]{3,2,1,0:T(8,128)(2,1)} %broadcast_in_dim.12), calls=%async_computation | async-start | bytes 4194304 | tf_op jit(solution)/shard_map/all_to_all | solution.py:17
  98.6 3.8 %collective-permute-start.2 = (bf16[2,512,256]{2,1,0:T(8,128)(2,1)}, bf16[2,512,256]{2,1,0:T(8,128)(2,1)}, u32[]{:S(2)}, u32[]{:S(2)}) collective-permute-start(bf16[2,512,256]{2,1,0:T(8,128)(2,1)} %copy-done.2), channel_id=1, source_target_pairs={{0,256},{256,0},{1,257},{257,1},{2,258},{258,2},{3,259},{259,3},{4... | collective-permute-start | bytes 1572872 | tf_op jit(solution)/shard_map/ppermute | solution.py:21
  102.4 6.9 %collective-permute-done.2 = bf16[2,512,256]{2,1,0:T(8,128)(2,1)} collective-permute-done((bf16[2,512,256]{2,1,0:T(8,128)(2,1)}, bf16[2,512,256]{2,1,0:T(8,128)(2,1)}, u32[]{:S(2)}, u32[]{:S(2)}) %collective-permute-start.2) | collective-permute-done | bytes 524320 | tf_op jit(solution)/shard_map/ppermute | solution.py:21
  109.3 5.5 %all-to-all-done.vg0_ref = bf16[4,2,512,256]{3,2,1,0:T(8,128)(2,1)S(1)} async-done(((bf16[4,2,512,256]{3,2,1,0:T(8,128)(2,1)}), bf16[4,2,512,256]{3,2,1,0:T(8,128)(2,1)S(1)}, u32[]{:S(2)}, u32[]{:S(2)}) %all-to-all-start) | async-done | bytes 2097184 | tf_op jit(solution)/shard_map/all_to_all | solution.py:17
  114.8 2.5 %broadcast_in_dim.13 = bf16[4,2,512,256]{3,2,1,0:T(8,128)(2,1)} broadcast(bf16[2,512,256]{2,1,0:T(8,128)(2,1)} %collective-permute-done.2), dimensions={1,2,3} | broadcast | bytes 2621440 | tf_op jit(solution)/shard_map/broadcast_in_dim | solution.py:17
  117.3 4.5 %all-to-all-start.1 = ((bf16[4,2,512,256]{3,2,1,0:T(8,128)(2,1)}), bf16[4,2,512,256]{3,2,1,0:T(8,128)(2,1)}, u32[]{:S(2)}, u32[]{:S(2)}) async-start(bf16[4,2,512,256]{3,2,1,0:T(8,128)(2,1)} %broadcast_in_dim.13), calls=%async_computation.1 | async-start | bytes 4194304 | tf_op jit(solution)/shard_map/all_to_all | solution.py:17
  121.9 3.8 %collective-permute-start.4 = (bf16[4,512,256]{2,1,0:T(8,128)(2,1)S(1)}, bf16[4,512,256]{2,1,0:T(8,128)(2,1)}, u32[]{:S(2)}, u32[]{:S(2)}) collective-permute-start(bf16[4,512,256]{2,1,0:T(8,128)(2,1)S(1)} %all-to-all-done.2), channel_id=1, source_target_pairs={{0,256},{256,0},{1,257},{257,1},{2,258},{258,2},{3,259},{259,3},{4... | collective-permute-start | bytes 3145736 | tf_op jit(solution)/shard_map/ppermute | solution.py:21
  125.6 13.4 %collective-permute-start.1 = (bf16[4,2,512,256]{3,2,1,0:T(8,128)(2,1)S(1)}, bf16[4,2,512,256]{3,2,1,0:T(8,128)(2,1)}, u32[]{:S(2)}, u32[]{:S(2)}) collective-permute-start(bf16[4,2,512,256]{3,2,1,0:T(8,128)(2,1)S(1)} %all-to-all-done.vg0_ref), channel_id=1, source_target_pairs={{0,1},{1,0},{2,3},{3,2},{4,5},{5,4},{6,7},{7,6},{8,9},{9,8},{10,11... | collective-permute-start | bytes 6291464 | tf_op jit(solution)/shard_map/ppermute | solution.py:21
  139.0 12.4 %collective-permute-start.3 = (bf16[4,2,512,256]{3,2,1,0:T(8,128)(2,1)}, bf16[4,2,512,256]{3,2,1,0:T(8,128)(2,1)}, u32[]{:S(2)}, u32[]{:S(2)}) collective-permute-start(bf16[4,2,512,256]{3,2,1,0:T(8,128)(2,1)} %all-to-all-done.1.vg0_ref), channel_id=1, source_target_pairs={{0,1},{1,0},{2,3},{3,2},{4,5},{5,4},{6,7},{7,6},{8,9},{9,8},{10,11... | collective-permute-start | bytes 6291464 | tf_op jit(solution)/shard_map/ppermute | solution.py:21
  151.5 2.8 %pad_maximum_fusion.o0_ref = bf16[2,4,512,256]{3,2,1,0:T(8,128)(2,1)} fusion(bf16[1,4,512,256]{3,2,1,0:T(8,128)(2,1)} %bitcast.20, bf16[1,4,512,256]{3,2,1,0:T(8,128)(2,1)S(1)} %bitcast.38), kind=kLoop, calls=%fused_computation | loop fusion | flops 1048576 | bytes 4194304 | tf_op jit(solution)/shard_map/stack | solution.py:141
  154.3 2.1 %collective-permute-start.5 = (bf16[2,4,512,256]{3,2,1,0:T(8,128)(2,1)}, bf16[2,4,512,256]{3,2,1,0:T(8,128)(2,1)}, u32[]{:S(2)}, u32[]{:S(2)}) collective-permute-start(bf16[2,4,512,256]{3,2,1,0:T(8,128)(2,1)} %pad_maximum_fusion.o0_ref), channel_id=1, source_target_pairs={{0,1},{1,0},{2,3},{3,2},{4,5},{5,4},{6,7},{7,6},{8,9},{9,8},{10,11... | collective-permute-start | bytes 6291464 | tf_op jit(solution)/shard_map/ppermute | solution.py:21
  156.3 3.7 %collective-permute-start = (bf16[32,2048]{1,0:T(8,128)(2,1)S(1)}, bf16[32,2048]{1,0:T(8,128)(2,1)S(1)}, u32[]{:S(2)}, u32[]{:S(2)}) collective-permute-start(bf16[32,2048]{1,0:T(8,128)(2,1)S(1)} %slice_bitcast_fusion.1), channel_id=1, source_target_pairs={{0,8},{8,16},{16,24},{24,32},{32,40},{40,48},{48,56},{56,64},{64,7... | collective-permute-start | bytes 393224 | tf_op jit(solution)/shard_map/ppermute | solution.py:134
  160.1 1.0 copy.20
  162.2 1.4 copy-done
  163.6 5.9 %shard_map.73 = (bf16[384,512]{1,0:T(8,128)(2,1)S(1)}, f32[2,384,128]{2,1,0:T(8,128)S(1)}) custom-call(s32[2]{0:T(128)S(1)} %pad_add_fusion.where_ref, bf16[32,2048]{1,0:T(8,128)(2,1)S(1)} %collective-permute-done.halo_ref, bf16[384,2048]{1,0:T(8,128)(2,1)S(1)} %bitcast.36, f32[2,31,512]{2,1,0:T(8,128)S(1)} %copy.22.cw_ref, ...), custom_call_target="tpu_custom_call" | custom-call | flops 1610612736 | bytes 8388608 | tf_op jit(solution)/shard_map/pallas_call | solution.py:101
  169.5 6.4 %shard_map.74 = (bf16[384,512]{1,0:T(8,128)(2,1)S(1)}, f32[2,384,128]{2,1,0:T(8,128)S(1)}) custom-call(s32[2]{0:T(128)S(1)} %pad_add_fusion.1.where_ref, bf16[32,2048]{1,0:T(8,128)(2,1)S(1)} %collective-permute-done.halo_ref, bf16[384,2048]{1,0:T(8,128)(2,1)S(1)} %bitcast.37, f32[2,31,512]{2,1,0:T(8,128)S(1)} %copy.22.cw_ref, ...), custom_call_target="tpu_custom_call" | custom-call | flops 1610612736 | bytes 8388608 | tf_op jit(solution)/shard_map/pallas_call | solution.py:101
  175.9 5.6 %shard_map.75 = bf16[384,2048]{1,0:T(8,128)(2,1)} custom-call(s32[2]{0:T(128)S(1)} %pad_add_fusion.where_ref, bf16[384,512]{1,0:T(8,128)(2,1)S(1)} %get-tuple-element.17.conv_a_ref, bf16[384,512]{1,0:T(8,128)(2,1)S(1)} %get-tuple-element.18.conv_b_ref, f32[2,384,128]{2,1,0:T(8,128)S(1)} %get-tuple-element.19.stats_a_ref, ...), custom_call_target="tpu_custom_call" | custom-call | flops 1610612736 | bytes 8388608 | tf_op jit(solution)/shard_map/pallas_call | solution.py:101
  (29 shorter events, 2.0 us)
Async XLA Ops:
  79.6 13.9 %all-to-all-start.2 = ((bf16[4,512,256]{2,1,0:T(8,128)(2,1)}), bf16[4,512,256]{2,1,0:T(8,128)(2,1)S(1)}, u32[]{:S(2)}, u32[]{:S(2)}) async-start(bf16[4,512,256]{2,1,0:T(8,128)(2,1)} %broadcast_in_dim.14), calls=%async_computation.2 | async-start | bytes 2097152 | tf_op jit(solution)/shard_map/all_to_all | solution.py:17
  83.7 11.2 %copy-start.2 = (bf16[2,512,256]{2,1,0:T(8,128)(2,1)}, bf16[2,512,256]{2,1,0:T(8,128)(2,1)S(1)}, u32[]{:S(2)}) copy-start(bf16[2,512,256]{2,1,0:T(8,128)(2,1)S(1)} %slice.14) | copy-start | bytes 1572868
  94.9 19.8 %all-to-all-start = ((bf16[4,2,512,256]{3,2,1,0:T(8,128)(2,1)}), bf16[4,2,512,256]{3,2,1,0:T(8,128)(2,1)S(1)}, u32[]{:S(2)}, u32[]{:S(2)}) async-start(bf16[4,2,512,256]{3,2,1,0:T(8,128)(2,1)} %broadcast_in_dim.12), calls=%async_computation | async-start | bytes 4194304 | tf_op jit(solution)/shard_map/all_to_all | solution.py:17
  98.6 10.7 %collective-permute-start.2 = (bf16[2,512,256]{2,1,0:T(8,128)(2,1)}, bf16[2,512,256]{2,1,0:T(8,128)(2,1)}, u32[]{:S(2)}, u32[]{:S(2)}) collective-permute-start(bf16[2,512,256]{2,1,0:T(8,128)(2,1)} %copy-done.2), channel_id=1, source_target_pairs={{0,256},{256,0},{1,257},{257,1},{2,258},{258,2},{3,259},{259,3},{4... | collective-permute-start | bytes 1572872 | tf_op jit(solution)/shard_map/ppermute | solution.py:21
  117.3 21.7 %all-to-all-start.1 = ((bf16[4,2,512,256]{3,2,1,0:T(8,128)(2,1)}), bf16[4,2,512,256]{3,2,1,0:T(8,128)(2,1)}, u32[]{:S(2)}, u32[]{:S(2)}) async-start(bf16[4,2,512,256]{3,2,1,0:T(8,128)(2,1)} %broadcast_in_dim.13), calls=%async_computation.1 | async-start | bytes 4194304 | tf_op jit(solution)/shard_map/all_to_all | solution.py:17
  121.9 29.6 %collective-permute-start.4 = (bf16[4,512,256]{2,1,0:T(8,128)(2,1)S(1)}, bf16[4,512,256]{2,1,0:T(8,128)(2,1)}, u32[]{:S(2)}, u32[]{:S(2)}) collective-permute-start(bf16[4,512,256]{2,1,0:T(8,128)(2,1)S(1)} %all-to-all-done.2), channel_id=1, source_target_pairs={{0,256},{256,0},{1,257},{257,1},{2,258},{258,2},{3,259},{259,3},{4... | collective-permute-start | bytes 3145736 | tf_op jit(solution)/shard_map/ppermute | solution.py:21
  125.6 36.5 %collective-permute-start.1 = (bf16[4,2,512,256]{3,2,1,0:T(8,128)(2,1)S(1)}, bf16[4,2,512,256]{3,2,1,0:T(8,128)(2,1)}, u32[]{:S(2)}, u32[]{:S(2)}) collective-permute-start(bf16[4,2,512,256]{3,2,1,0:T(8,128)(2,1)S(1)} %all-to-all-done.vg0_ref), channel_id=1, source_target_pairs={{0,1},{1,0},{2,3},{3,2},{4,5},{5,4},{6,7},{7,6},{8,9},{9,8},{10,11... | collective-permute-start | bytes 6291464 | tf_op jit(solution)/shard_map/ppermute | solution.py:21
  139.0 30.4 %collective-permute-start.3 = (bf16[4,2,512,256]{3,2,1,0:T(8,128)(2,1)}, bf16[4,2,512,256]{3,2,1,0:T(8,128)(2,1)}, u32[]{:S(2)}, u32[]{:S(2)}) collective-permute-start(bf16[4,2,512,256]{3,2,1,0:T(8,128)(2,1)} %all-to-all-done.1.vg0_ref), channel_id=1, source_target_pairs={{0,1},{1,0},{2,3},{3,2},{4,5},{5,4},{6,7},{7,6},{8,9},{9,8},{10,11... | collective-permute-start | bytes 6291464 | tf_op jit(solution)/shard_map/ppermute | solution.py:21
  154.3 7.1 %copy-start.3 = (f32[1024]{0:T(1024)S(1)}, f32[1024]{0:T(1024)}, u32[]{:S(2)}) copy-start(f32[1024]{0:T(1024)} %param.11) | copy-start | bytes 12292
  154.3 7.3 %copy-start.4 = (f32[1024]{0:T(1024)S(1)}, f32[1024]{0:T(1024)}, u32[]{:S(2)}) copy-start(f32[1024]{0:T(1024)} %param.12) | copy-start | bytes 12292
  154.3 21.7 %collective-permute-start.5 = (bf16[2,4,512,256]{3,2,1,0:T(8,128)(2,1)}, bf16[2,4,512,256]{3,2,1,0:T(8,128)(2,1)}, u32[]{:S(2)}, u32[]{:S(2)}) collective-permute-start(bf16[2,4,512,256]{3,2,1,0:T(8,128)(2,1)} %pad_maximum_fusion.o0_ref), channel_id=1, source_target_pairs={{0,1},{1,0},{2,3},{3,2},{4,5},{5,4},{6,7},{7,6},{8,9},{9,8},{10,11... | collective-permute-start | bytes 6291464 | tf_op jit(solution)/shard_map/ppermute | solution.py:21
  156.3 5.8 %collective-permute-start = (bf16[32,2048]{1,0:T(8,128)(2,1)S(1)}, bf16[32,2048]{1,0:T(8,128)(2,1)S(1)}, u32[]{:S(2)}, u32[]{:S(2)}) collective-permute-start(bf16[32,2048]{1,0:T(8,128)(2,1)S(1)} %slice_bitcast_fusion.1), channel_id=1, source_target_pairs={{0,8},{8,16},{16,24},{24,32},{32,40},{40,48},{48,56},{56,64},{64,7... | collective-permute-start | bytes 393224 | tf_op jit(solution)/shard_map/ppermute | solution.py:134
  162.2 1.4 copy-start
  163.6 5.9 %copy-start.1 = (bf16[1,384,2048]{2,1,0:T(8,128)(2,1)S(1)}, bf16[1,384,2048]{2,1,0:T(8,128)(2,1)}, u32[]{:S(2)}) copy-start(bf16[1,384,2048]{2,1,0:T(8,128)(2,1)} %param.7) | copy-start | bytes 4718596

commit v2 on v1

--- a/solution.py
+++ b/solution.py
@@ -27,26 +27,38 @@
     return pl.ds(pl.multiple_of((2 * x + c) * deep, deep), deep)
 
 
-def convolve(where_ref, halo_ref, tok_ref, cw_ref, vg0_ref, vg1_ref, conv_ref, stats_ref, tok, shifted):
+def chosen(array, par, precision=None):
+    wide, width = 2 * LANES, LANES // 8
+    source = lax.broadcasted_iota(jnp.int32, (wide, LANES), 0)
+    target = lax.broadcasted_iota(jnp.int32, (wide, LANES), 1)
+    pick = source == (target // width) * (2 * width) + par * width + target % width
+    pick = jnp.where(pick, 1.0, 0.0).astype(array.dtype)
+    parts = [array[:, at : at + wide] for at in range(0, array.shape[1], wide)]
+    parts = [jnp.dot(p, pick, preferred_element_type=jnp.float32, precision=precision) for p in parts]
+    return jnp.concatenate(parts, axis=1)
+
+
+def convolve(where_ref, halo_ref, tok_ref, cw_ref, v0_ref, v1_ref, g0_ref, g1_ref, conv_ref, stats_ref, tok, shifted, cw):
     par = where_ref[1]
     rows, part = conv_ref.shape
-    taps = cw_ref.shape[1]
-    blocks, deep = vg0_ref.shape[0], vg0_ref.shape[-1]
+    taps = cw_ref.shape[0]
+    blocks, deep = v0_ref.shape[0], v0_ref.shape[-1]
     order = [(x, m) for x in range(blocks) for m in range(2)]
     for at, (x, m) in enumerate(order):
         here = slice(at * deep, (at + 1) * deep)
         tok[:HALO, here] = halo_ref[:, columns(where_ref, x, m, deep)]
         tok[HALO:, here] = tok_ref[:, columns(where_ref, x, m, deep)]
+    cw[...] = chosen(cw_ref[...], par)
 
     half = rows // 2
     for q in range(part // PIECE):
         span = slice(q * PIECE, (q + 1) * PIECE)
 
-        def product(m):
-            piece = jnp.concatenate([(vg0_ref, vg1_ref)[c][x, m, span, :] for x, c in order], axis=1)
+        def product(*refs):
+            piece = jnp.concatenate([refs[m][x, span, :] for x, m in order], axis=1)
             return lax.dot_general(tok[...], piece, (((1,), (1,)), ((), ())), preferred_element_type=jnp.float32)
 
-        value, gate = product(0), product(1)
+        value, gate = product(v0_ref, v1_ref), product(g0_ref, g1_ref)
         glu = (value * jax.nn.sigmoid(gate)).astype(jnp.bfloat16).astype(jnp.float32)
         shifted[0] = glu
         for r in range(1, 8):
@@ -59,7 +71,7 @@
                 for k in range(taps):
                     r, j = k % 8, k // 8
                     begin = HALO - 8 * j + h * half
-                    acc = acc + cw_ref[par, k : k + 1, at : at + LANES] * shifted[r, begin : begin + half, lanes]
+                    acc = acc + cw[k : k + 1, at : at + LANES] * shifted[r, begin : begin + half, lanes]
                 acc = acc.astype(jnp.bfloat16)
                 when = slice(h * half, (h + 1) * half)
                 conv_ref[when, at : at + LANES] = acc
@@ -72,23 +84,28 @@
                     stats_ref[1, when] += acc * acc
 
 
-def finish(where_ref, conv_a_ref, conv_b_ref, stats_a_ref, stats_b_ref, gain_ref, bias_ref, o0_ref, o1_ref, out_ref, normed):
+def finish(
+    where_ref, conv_a_ref, conv_b_ref, stats_a_ref, stats_b_ref, gain_ref, bias_ref,
+    oa0_ref, ob0_ref, oa1_ref, ob1_ref, out_ref, normed,
+):
     side = where_ref[1]
     part = conv_a_ref.shape[1]
-    blocks, deep = o0_ref.shape[1], o0_ref.shape[-1]
+    blocks, deep = oa0_ref.shape[0], oa0_ref.shape[-1]
     mean = jnp.sum(stats_a_ref[0] + stats_b_ref[0], axis=1, keepdims=True) / (2 * part)
     meansq = jnp.sum(stats_a_ref[1] + stats_b_ref[1], axis=1, keepdims=True) / (2 * part)
     scale = lax.rsqrt(meansq - mean * mean + EPS)
     for s, conv_ref in enumerate((conv_a_ref, conv_b_ref)):
         par = side if s == 0 else 1 - side
+        gain = chosen(jnp.broadcast_to(gain_ref[...], (8, 2 * part)), par, lax.Precision.HIGHEST)[:1]
+        bias = chosen(jnp.broadcast_to(bias_ref[...], (8, 2 * part)), par, lax.Precision.HIGHEST)[:1]
         for q in range(part // PIECE):
             span = slice(q * PIECE, (q + 1) * PIECE)
-            v = (conv_ref[:, span].astype(jnp.float32) - mean) * scale * gain_ref[par, :, span] + bias_ref[par, :, span]
+            v = (conv_ref[:, span].astype(jnp.float32) - mean) * scale * gain[:, span] + bias[:, span]
             here = slice(s * part + q * PIECE, s * part + (q + 1) * PIECE)
             normed[:, here] = (v / (1.0 + jnp.exp(-v))).astype(jnp.bfloat16)
     for x in range(blocks):
-        for m, o_ref in enumerate((o0_ref, o1_ref)):
-            right = jnp.concatenate([o_ref[0, x], o_ref[1, x]], axis=0)
+        for m, (own, other) in enumerate(((oa0_ref, ob0_ref), (oa1_ref, ob1_ref))):
+            right = jnp.concatenate([own[x], other[x]], axis=0)
             out = jnp.dot(normed[...], right, preferred_element_type=jnp.float32)
             out_ref[:, columns(where_ref, x, m, deep)] = out.astype(jnp.bfloat16)
 
@@ -107,11 +124,6 @@
         compiler_params=pltpu.CompilerParams(vmem_limit_bytes=mib * 1024 * 1024),
         cost_estimate=pl.CostEstimate(flops=flops, bytes_accessed=8 * 1024 * 1024, transcendentals=0),
     )(*operands)
-
-
-def by_side(array, positions):
-    k = array.shape[0]
-    return array.reshape(k, positions, 2, -1).transpose(2, 0, 1, 3).reshape(2, k, -1)
 
 
 def per_device(tokens, w_value, w_gate, conv_weight, norm_gain, norm_bias, w_out):
@@ -129,33 +141,37 @@
     near = near.transpose(2, 1, 0, 3, 4).reshape(3, positions * half, -1)
     last = rows[length - HALO :]
     near, last, conv_weight, norm_gain, norm_bias = lax.optimization_barrier((near, last, conv_weight, norm_gain, norm_bias))
-    vg, o = near[:2], near[2]
-    vg_other = swapped(vg, "side")
+    v, g, o = near
+
+    ga0 = spread(g, "x")
+    v_other = swapped(v, "side")
     halo = lax.ppermute(last, ("zh", "zl"), [(i, i + 1) for i in range(positions - 1)])
-    oa = spread(o, "x")
-    ob = swapped(oa, "side")
-    vga0 = spread(vg, "x")
-    vga1 = swapped(vga0, "core")
-    vgb0 = spread(vg_other, "x")
-    vgb1 = swapped(vgb0, "core")
-    o0 = jnp.stack([oa, ob])
-    o1 = swapped(o0, "core")
-    taps = by_side(conv_weight.astype(jnp.float32), positions)
-    gain, bias = by_side(norm_gain[None], positions), by_side(norm_bias[None], positions)
+    oa0 = spread(o, "x")
+    gb0 = swapped(ga0, "side")
+    ga1 = swapped(ga0, "core")
+    va0 = spread(v, "x")
+    ob0 = swapped(oa0, "side")
+    oa1 = swapped(oa0, "core")
+    vb0 = spread(v_other, "x")
+    va1 = swapped(va0, "core")
+    gb1 = swapped(gb0, "core")
+    vb1 = swapped(vb0, "core")
+    ob1 = swapped(ob0, "core")
     here, there = (jnp.stack([core, s]).astype(jnp.int32) for s in (side, 1 - side))
     part = channels // 2
     made = (jax.ShapeDtypeStruct((length, part), jnp.bfloat16), jax.ShapeDtypeStruct((2, length, LANES), jnp.float32))
     scratch = [
         pltpu.VMEM((length + HALO, depth), jnp.bfloat16),
         pltpu.VMEM((8, length + HALO, PIECE), jnp.float32),
+        pltpu.VMEM((conv_weight.shape[0], part), jnp.float32),
     ]
     flops = 2 * length * depth * channels
-    conv_a, stats_a = kernel(convolve, made, scratch, flops, 20, here, halo, rows, taps, vga0, vga1)
-    conv_b, stats_b = kernel(convolve, made, scratch, flops, 20, there, halo, rows, taps, vgb0, vgb1)
+    conv_a, stats_a = kernel(convolve, made, scratch, flops, 20, here, halo, rows, conv_weight, va0, va1, ga0, ga1)
+    conv_b, stats_b = kernel(convolve, made, scratch, flops, 20, there, halo, rows, conv_weight, vb0, vb1, gb0, gb1)
     mixed = kernel(
         finish, jax.ShapeDtypeStruct((length, depth), jnp.bfloat16),
         [pltpu.VMEM((length, channels), jnp.bfloat16)], flops, 16,
-        here, conv_a, conv_b, stats_a, stats_b, gain, bias, o0, o1,
+        here, conv_a, conv_b, stats_a, stats_b, norm_gain[None], norm_bias[None], oa0, ob0, oa1, ob1,
     )
     return mixed[None]
 

time: 182 us -> 192 us (1.055)
  blocking collectives: 76.7 us -> 106 us
  waiting for transfers between devices: 22.4 us -> 4.52 us
  starting transfers between devices: 51.5 us -> 57.1 us
  local copies, waits for them, and re-layouts: 9.15 us -> 4.85 us
  other arithmetic: 3.66 us -> 0.88 us
    all_to_all x0 -> x2, blocking collectives: none -> 28.7 us  [spread(): lax.all_to_all(jnp.broadcast_to(block, (members, *block.shape)), axis, 0, 0)]
    all_to_all x3 -> x2, waiting for transfers between devices: 15.2 us -> 1.68 us  [spread(): lax.all_to_all(jnp.broadcast_to(block, (members, *block.shape)), axis, 0, 0)]
    ppermute x5 -> x9, starting transfers between devices: 35.4 us -> 46.3 us  [swapped(): return lax.ppermute(array, axis, [(0, 1), (1, 0)])]
    ppermute x5 -> x9, waiting for transfers between devices: 6.88 us -> 0.02 us  [swapped(): return lax.ppermute(array, axis, [(0, 1), (1, 0)])]
    all_to_all x3 -> x2, starting transfers between devices: 12.4 us -> 8.02 us  [spread(): lax.all_to_all(jnp.broadcast_to(block, (members, *block.shape)), axis, 0, 0)]
    broadcast_in_dim x3 -> x4, local copies, waits for them, and re-layouts: 5.05 us -> 2.21 us  [spread(): jnp.broadcast_to(block, (members, *block.shape))]
    another operation x1 -> x0, other arithmetic: 2.78 us -> none  [per_device(): o0 = jnp.stack([oa, ob])]
    ppermute x1, waiting for transfers between devices: 0.34 us -> 2.81 us  [per_device(): lax.ppermute(last, ('zh', 'zl'), [(i, i + 1) for i in range(positions - 1)])]
  transfers between devices with their start and end apart: 9 -> 12, of which waited for: 4 -> 2; matrix products, arithmetic and copies ran while one was open for 3% -> 1% of each run, Pallas kernels for 7% -> 6%
where the time goes in v2:
time: 192 us; the launch traced here: 191 us
  blocking collectives  106 us (55%)
  starting transfers between devices  57.1 us (30%)
  Pallas kernels  17.9 us (9%)
  local copies, waits for them, and re-layouts  4.85 us (3%)
  waiting for transfers between devices  4.52 us (2%)
    all_gather x1, blocking collectives, per_device(): far = lax.all_gather(mine, 'zh', axis=0, tiled=True)  69.2 us
    ppermute x9, starting transfers between devices, swapped(): return lax.ppermute(array, axis, [(0, 1), (1, 0)])  46.3 us
    all_to_all x2, blocking collectives, spread(): lax.all_to_all(jnp.broadcast_to(block, (members, *block.shape)), axis, 0, 0)  28.7 us
    pallas_call x3, Pallas kernels, kernel(): pl.pallas_call(function, out_shape=out_shape, in_specs=[SMEM] + [VMEM] *...  17.9 us
    all_to_all x2, starting transfers between devices, spread(): lax.all_to_all(jnp.broadcast_to(block, (members, *block.shape)), axis, 0, 0)  8.02 us
    all_gather x1, blocking collectives, per_device(): near = lax.all_gather(far, 'zl', axis=0, tiled=True)  7.68 us
  transfers between devices with their start and end apart: 12, of which 2 were waited for; matrix products, arithmetic and copies ran while one was open for 1% of the time, Pallas kernels for 6%

profile of v2, /device:TPU:33, one launch (start us, length us, event | category | flops | bytes accessed | tf_op | source)
XLA Modules:
  0.0 191.0 jit_solution(9111772160569325126)
XLA Ops:
  0.7 69.2 %all_gather.6 = bf16[48,16,256]{2,1,0:T(8,128)(2,1)S(1)} all-gather(bf16[3,16,256]{2,1,0:T(8,128)(2,1)S(1)} %fusion.1), channel_id=1, replica_groups=mesh['pair'=1,'side'=2,'zh'=16,'zl'=2,'x'=4,'core'=2] {'zh'}, dimensions={0}, use_global_device_ids=true | all-gather | bytes 417792 | tf_op jit(solution)/shard_map/all_gather | solution.py:138
  69.9 7.7 %all_gather.7 = bf16[96,16,256]{2,1,0:T(8,128)(2,1)S(1)} all-gather(bf16[48,16,256]{2,1,0:T(8,128)(2,1)S(1)} %all_gather.6), channel_id=1, replica_groups=mesh['pair'=1,'side'=2,'zh'=16,'zl'=2,'x'=4,'core'=2] {'zl'}, dimensions={0}, use_global_device_ids=true | all-gather | bytes 1179648 | tf_op jit(solution)/shard_map/all_gather | solution.py:139
  77.9 13.8 %all_to_all.20.g0_ref = bf16[4,512,256]{2,1,0:T(8,128)(2,1)} all-to-all(bf16[4,512,256]{2,1,0:T(8,128)(2,1)S(1)} %broadcast_in_dim.22), channel_id=1, replica_groups=mesh['pair'=1,'side'=2,'zh'=16,'zl'=2,'x'=4,'core'=2] {'x'}, dimensions={0} | all-to-all | bytes 2097152 | tf_op jit(solution)/shard_map/all_to_all | solution.py:17
  91.7 14.9 %all_to_all.21.v0_ref = bf16[4,512,256]{2,1,0:T(8,128)(2,1)} all-to-all(bf16[4,512,256]{2,1,0:T(8,128)(2,1)S(1)} %broadcast_in_dim.21), channel_id=1, replica_groups=mesh['pair'=1,'side'=2,'zh'=16,'zl'=2,'x'=4,'core'=2] {'x'}, dimensions={0} | all-to-all | bytes 2097152 | tf_op jit(solution)/shard_map/all_to_all | solution.py:17
  107.6 3.6 %all-to-all-start.3 = ((bf16[4,512,256]{2,1,0:T(8,128)(2,1)}), bf16[4,512,256]{2,1,0:T(8,128)(2,1)S(1)}, u32[]{:S(2)}, u32[]{:S(2)}) async-start(bf16[4,512,256]{2,1,0:T(8,128)(2,1)} %broadcast_in_dim.26), calls=%async_computation.3 | async-start | bytes 2097152 | tf_op jit(solution)/shard_map/all_to_all | solution.py:17
  111.3 3.9 %collective-permute-start.3 = (bf16[512,256]{1,0:T(8,128)(2,1)S(1)}, bf16[512,256]{1,0:T(8,128)(2,1)S(1)}, u32[]{:S(2)}, u32[]{:S(2)}) collective-permute-start(bf16[512,256]{1,0:T(8,128)(2,1)S(1)} %get-tuple-element.25), channel_id=1, source_target_pairs={{0,256},{256,0},{1,257},{257,1},{2,258},{258,2},{3,259},{259,3},{4... | collective-permute-start | bytes 786440 | tf_op jit(solution)/shard_map/ppermute | solution.py:21
  115.2 2.0 %collective-permute-start.5 = (bf16[4,512,256]{2,1,0:T(8,128)(2,1)}, bf16[4,512,256]{2,1,0:T(8,128)(2,1)}, u32[]{:S(2)}, u32[]{:S(2)}) collective-permute-start(bf16[4,512,256]{2,1,0:T(8,128)(2,1)} %all_to_all.20.g0_ref), channel_id=1, source_target_pairs={{0,256},{256,0},{1,257},{257,1},{2,258},{258,2},{3,259},{259,3},{4... | collective-permute-start | bytes 3145736 | tf_op jit(solution)/shard_map/ppermute | solution.py:21
  117.2 15.1 %collective-permute-start.1 = (bf16[4,512,256]{2,1,0:T(8,128)(2,1)}, bf16[4,512,256]{2,1,0:T(8,128)(2,1)}, u32[]{:S(2)}, u32[]{:S(2)}) collective-permute-start(bf16[4,512,256]{2,1,0:T(8,128)(2,1)} %all_to_all.21.v0_ref), channel_id=1, source_target_pairs={{0,1},{1,0},{2,3},{3,2},{4,5},{5,4},{6,7},{7,6},{8,9},{9,8},{10,11... | collective-permute-start | bytes 3145736 | tf_op jit(solution)/shard_map/ppermute | solution.py:21
  132.2 3.7 %collective-permute-start.7 = (bf16[4,512,256]{2,1,0:T(8,128)(2,1)S(1)}, bf16[4,512,256]{2,1,0:T(8,128)(2,1)}, u32[]{:S(2)}, u32[]{:S(2)}) collective-permute-start(bf16[4,512,256]{2,1,0:T(8,128)(2,1)S(1)} %all-to-all-done.3.oa0_ref), channel_id=1, source_target_pairs={{0,256},{256,0},{1,257},{257,1},{2,258},{258,2},{3,259},{259,3},{4... | collective-permute-start | bytes 3145736 | tf_op jit(solution)/shard_map/ppermute | solution.py:21
  135.9 1.0 broadcast_in_dim.23
  137.0 4.4 %all-to-all-start.2 = ((bf16[4,512,256]{2,1,0:T(8,128)(2,1)}), bf16[4,512,256]{2,1,0:T(8,128)(2,1)}, u32[]{:S(2)}, u32[]{:S(2)}) async-start(bf16[4,512,256]{2,1,0:T(8,128)(2,1)} %broadcast_in_dim.23), calls=%async_computation.2 | async-start | bytes 2097152 | tf_op jit(solution)/shard_map/all_to_all | solution.py:17
  141.4 4.9 %collective-permute-start.2 = (bf16[4,512,256]{2,1,0:T(8,128)(2,1)}, bf16[4,512,256]{2,1,0:T(8,128)(2,1)}, u32[]{:S(2)}, u32[]{:S(2)}) collective-permute-start(bf16[4,512,256]{2,1,0:T(8,128)(2,1)} %all_to_all.20.g0_ref), channel_id=1, source_target_pairs={{0,1},{1,0},{2,3},{3,2},{4,5},{5,4},{6,7},{7,6},{8,9},{9,8},{10,11... | collective-permute-start | bytes 3145736 | tf_op jit(solution)/shard_map/ppermute | solution.py:21
  146.3 2.7 %collective-permute-start = (bf16[32,2048]{1,0:T(8,128)(2,1)S(1)}, bf16[32,2048]{1,0:T(8,128)(2,1)S(1)}, u32[]{:S(2)}, u32[]{:S(2)}) collective-permute-start(bf16[32,2048]{1,0:T(8,128)(2,1)S(1)} %slice_bitcast_fusion.3), channel_id=1, source_target_pairs={{0,8},{8,16},{16,24},{24,32},{32,40},{40,48},{48,56},{56,64},{64,7... | collective-permute-start | bytes 393224 | tf_op jit(solution)/shard_map/ppermute | solution.py:148
  149.0 2.8 %collective-permute-done.halo_ref = bf16[32,2048]{1,0:T(8,128)(2,1)S(1)} collective-permute-done((bf16[32,2048]{1,0:T(8,128)(2,1)S(1)}, bf16[32,2048]{1,0:T(8,128)(2,1)S(1)}, u32[]{:S(2)}, u32[]{:S(2)}) %collective-permute-start) | collective-permute-done | bytes 131104 | tf_op jit(solution)/shard_map/ppermute | solution.py:148
  151.9 1.7 all-to-all-done.2.v0_ref
  153.5 5.9 %collective-permute-start.4 = (bf16[4,512,256]{2,1,0:T(8,128)(2,1)}, bf16[4,512,256]{2,1,0:T(8,128)(2,1)}, u32[]{:S(2)}, u32[]{:S(2)}) collective-permute-start(bf16[4,512,256]{2,1,0:T(8,128)(2,1)} %all-to-all-done.2.v0_ref), channel_id=1, source_target_pairs={{0,1},{1,0},{2,3},{3,2},{4,5},{5,4},{6,7},{7,6},{8,9},{9,8},{10,11... | collective-permute-start | bytes 3145736 | tf_op jit(solution)/shard_map/ppermute | solution.py:21
  159.5 2.0 %collective-permute-start.6 = (bf16[4,512,256]{2,1,0:T(8,128)(2,1)}, bf16[4,512,256]{2,1,0:T(8,128)(2,1)}, u32[]{:S(2)}, u32[]{:S(2)}) collective-permute-start(bf16[4,512,256]{2,1,0:T(8,128)(2,1)} %collective-permute-done.5.g0_ref), channel_id=1, source_target_pairs={{0,1},{1,0},{2,3},{3,2},{4,5},{5,4},{6,7},{7,6},{8,9},{9,8},{10,11... | collective-permute-start | bytes 3145736 | tf_op jit(solution)/shard_map/ppermute | solution.py:21
  161.5 2.4 %collective-permute-start.8 = (bf16[4,512,256]{2,1,0:T(8,128)(2,1)S(1)}, bf16[4,512,256]{2,1,0:T(8,128)(2,1)}, u32[]{:S(2)}, u32[]{:S(2)}) collective-permute-start(bf16[4,512,256]{2,1,0:T(8,128)(2,1)S(1)} %all-to-all-done.3.oa0_ref), channel_id=1, source_target_pairs={{0,1},{1,0},{2,3},{3,2},{4,5},{5,4},{6,7},{7,6},{8,9},{9,8},{10,11... | collective-permute-start | bytes 3145736 | tf_op jit(solution)/shard_map/ppermute | solution.py:21
  163.9 6.5 %collective-permute-start.9 = (bf16[4,512,256]{2,1,0:T(8,128)(2,1)}, bf16[4,512,256]{2,1,0:T(8,128)(2,1)}, u32[]{:S(2)}, u32[]{:S(2)}) collective-permute-start(bf16[4,512,256]{2,1,0:T(8,128)(2,1)} %collective-permute-done.7.ob0_ref), channel_id=1, source_target_pairs={{0,1},{1,0},{2,3},{3,2},{4,5},{5,4},{6,7},{7,6},{8,9},{9,8},{10,11... | collective-permute-start | bytes 3145736 | tf_op jit(solution)/shard_map/ppermute | solution.py:21
  170.6 1.2 copy-done.1
  171.8 1.2 copy-done.2
  173.0 5.6 %shard_map.73 = (bf16[384,512]{1,0:T(8,128)(2,1)S(1)}, f32[2,384,128]{2,1,0:T(8,128)S(1)}) custom-call(s32[2]{0:T(128)S(1)} %pad_add_fusion.where_ref, bf16[32,2048]{1,0:T(8,128)(2,1)S(1)} %collective-permute-done.halo_ref, bf16[384,2048]{1,0:T(8,128)(2,1)S(1)} %bitcast.26, bf16[31,1024]{1,0:T(8,128)(2,1)S(1)} %copy-done.3, ...), custom_call_target="tpu_custom_call" | custom-call | flops 1610612736 | bytes 8388608 | tf_op jit(solution)/shard_map/pallas_call | solution.py:118
  178.7 6.3 %shard_map.74 = (bf16[384,512]{1,0:T(8,128)(2,1)S(1)}, f32[2,384,128]{2,1,0:T(8,128)S(1)}) custom-call(s32[2]{0:T(128)S(1)} %pad_add_fusion.1.where_ref, bf16[32,2048]{1,0:T(8,128)(2,1)S(1)} %collective-permute-done.halo_ref, bf16[384,2048]{1,0:T(8,128)(2,1)S(1)} %bitcast.27, bf16[31,1024]{1,0:T(8,128)(2,1)S(1)} %copy-done.3, ...), custom_call_target="tpu_custom_call" | custom-call | flops 1610612736 | bytes 8388608 | tf_op jit(solution)/shard_map/pallas_call | solution.py:118
  185.0 6.0 %shard_map.75 = bf16[384,2048]{1,0:T(8,128)(2,1)} custom-call(s32[2]{0:T(128)S(1)} %pad_add_fusion.where_ref, bf16[384,512]{1,0:T(8,128)(2,1)S(1)} %get-tuple-element.17.conv_a_ref, bf16[384,512]{1,0:T(8,128)(2,1)S(1)} %get-tuple-element.18.conv_b_ref, f32[2,384,128]{2,1,0:T(8,128)S(1)} %get-tuple-element.19.stats_a_ref, ...), custom_call_target="tpu_custom_call" | custom-call | flops 1610612736 | bytes 8388608 | tf_op jit(solution)/shard_map/pallas_call | solution.py:118
  (29 shorter events, 2.3 us)
Async XLA Ops:
  0.7 77.0 %copy-start = (bf16[1,384,2048]{2,1,0:T(8,128)(2,1)S(1)}, bf16[1,384,2048]{2,1,0:T(8,128)(2,1)}, u32[]{:S(2)}) copy-start(bf16[1,384,2048]{2,1,0:T(8,128)(2,1)} %param.7) | copy-start | bytes 4718596
  107.6 24.6 %all-to-all-start.3 = ((bf16[4,512,256]{2,1,0:T(8,128)(2,1)}), bf16[4,512,256]{2,1,0:T(8,128)(2,1)S(1)}, u32[]{:S(2)}, u32[]{:S(2)}) async-start(bf16[4,512,256]{2,1,0:T(8,128)(2,1)} %broadcast_in_dim.26), calls=%async_computation.3 | async-start | bytes 2097152 | tf_op jit(solution)/shard_map/all_to_all | solution.py:17
  111.3 59.3 %copy-start.3 = (bf16[31,1024]{1,0:T(8,128)(2,1)S(1)}, bf16[31,1024]{1,0:T(8,128)(2,1)}, u32[]{:S(2)}) copy-start(bf16[31,1024]{1,0:T(8,128)(2,1)} %cw_ref.1) | copy-start | bytes 190468
  111.3 24.7 %collective-permute-start.3 = (bf16[512,256]{1,0:T(8,128)(2,1)S(1)}, bf16[512,256]{1,0:T(8,128)(2,1)S(1)}, u32[]{:S(2)}, u32[]{:S(2)}) collective-permute-start(bf16[512,256]{1,0:T(8,128)(2,1)S(1)} %get-tuple-element.25), channel_id=1, source_target_pairs={{0,256},{256,0},{1,257},{257,1},{2,258},{258,2},{3,259},{259,3},{4... | collective-permute-start | bytes 786440 | tf_op jit(solution)/shard_map/ppermute | solution.py:21
  115.2 44.3 %collective-permute-start.5 = (bf16[4,512,256]{2,1,0:T(8,128)(2,1)}, bf16[4,512,256]{2,1,0:T(8,128)(2,1)}, u32[]{:S(2)}, u32[]{:S(2)}) collective-permute-start(bf16[4,512,256]{2,1,0:T(8,128)(2,1)} %all_to_all.20.g0_ref), channel_id=1, source_target_pairs={{0,256},{256,0},{1,257},{257,1},{2,258},{258,2},{3,259},{259,3},{4... | collective-permute-start | bytes 3145736 | tf_op jit(solution)/shard_map/ppermute | solution.py:21
  117.2 44.3 %collective-permute-start.1 = (bf16[4,512,256]{2,1,0:T(8,128)(2,1)}, bf16[4,512,256]{2,1,0:T(8,128)(2,1)}, u32[]{:S(2)}, u32[]{:S(2)}) collective-permute-start(bf16[4,512,256]{2,1,0:T(8,128)(2,1)} %all_to_all.21.v0_ref), channel_id=1, source_target_pairs={{0,1},{1,0},{2,3},{3,2},{4,5},{5,4},{6,7},{7,6},{8,9},{9,8},{10,11... | collective-permute-start | bytes 3145736 | tf_op jit(solution)/shard_map/ppermute | solution.py:21
  132.2 31.7 %collective-permute-start.7 = (bf16[4,512,256]{2,1,0:T(8,128)(2,1)S(1)}, bf16[4,512,256]{2,1,0:T(8,128)(2,1)}, u32[]{:S(2)}, u32[]{:S(2)}) collective-permute-start(bf16[4,512,256]{2,1,0:T(8,128)(2,1)S(1)} %all-to-all-done.3.oa0_ref), channel_id=1, source_target_pairs={{0,256},{256,0},{1,257},{257,1},{2,258},{258,2},{3,259},{259,3},{4... | collective-permute-start | bytes 3145736 | tf_op jit(solution)/shard_map/ppermute | solution.py:21
  137.0 16.6 %all-to-all-start.2 = ((bf16[4,512,256]{2,1,0:T(8,128)(2,1)}), bf16[4,512,256]{2,1,0:T(8,128)(2,1)}, u32[]{:S(2)}, u32[]{:S(2)}) async-start(bf16[4,512,256]{2,1,0:T(8,128)(2,1)} %broadcast_in_dim.23), calls=%async_computation.2 | async-start | bytes 2097152 | tf_op jit(solution)/shard_map/all_to_all | solution.py:17
  141.4 29.2 %collective-permute-start.2 = (bf16[4,512,256]{2,1,0:T(8,128)(2,1)}, bf16[4,512,256]{2,1,0:T(8,128)(2,1)}, u32[]{:S(2)}, u32[]{:S(2)}) collective-permute-start(bf16[4,512,256]{2,1,0:T(8,128)(2,1)} %all_to_all.20.g0_ref), channel_id=1, source_target_pairs={{0,1},{1,0},{2,3},{3,2},{4,5},{5,4},{6,7},{7,6},{8,9},{9,8},{10,11... | collective-permute-start | bytes 3145736 | tf_op jit(solution)/shard_map/ppermute | solution.py:21
  146.3 5.5 %collective-permute-start = (bf16[32,2048]{1,0:T(8,128)(2,1)S(1)}, bf16[32,2048]{1,0:T(8,128)(2,1)S(1)}, u32[]{:S(2)}, u32[]{:S(2)}) collective-permute-start(bf16[32,2048]{1,0:T(8,128)(2,1)S(1)} %slice_bitcast_fusion.3), channel_id=1, source_target_pairs={{0,8},{8,16},{16,24},{24,32},{32,40},{40,48},{48,56},{56,64},{64,7... | collective-permute-start | bytes 393224 | tf_op jit(solution)/shard_map/ppermute | solution.py:148
  153.5 25.2 %collective-permute-start.4 = (bf16[4,512,256]{2,1,0:T(8,128)(2,1)}, bf16[4,512,256]{2,1,0:T(8,128)(2,1)}, u32[]{:S(2)}, u32[]{:S(2)}) collective-permute-start(bf16[4,512,256]{2,1,0:T(8,128)(2,1)} %all-to-all-done.2.v0_ref), channel_id=1, source_target_pairs={{0,1},{1,0},{2,3},{3,2},{4,5},{5,4},{6,7},{7,6},{8,9},{9,8},{10,11... | collective-permute-start | bytes 3145736 | tf_op jit(solution)/shard_map/ppermute | solution.py:21
  159.5 19.2 %collective-permute-start.6 = (bf16[4,512,256]{2,1,0:T(8,128)(2,1)}, bf16[4,512,256]{2,1,0:T(8,128)(2,1)}, u32[]{:S(2)}, u32[]{:S(2)}) collective-permute-start(bf16[4,512,256]{2,1,0:T(8,128)(2,1)} %collective-permute-done.5.g0_ref), channel_id=1, source_target_pairs={{0,1},{1,0},{2,3},{3,2},{4,5},{5,4},{6,7},{7,6},{8,9},{9,8},{10,11... | collective-permute-start | bytes 3145736 | tf_op jit(solution)/shard_map/ppermute | solution.py:21
  161.5 23.5 %collective-permute-start.8 = (bf16[4,512,256]{2,1,0:T(8,128)(2,1)S(1)}, bf16[4,512,256]{2,1,0:T(8,128)(2,1)}, u32[]{:S(2)}, u32[]{:S(2)}) collective-permute-start(bf16[4,512,256]{2,1,0:T(8,128)(2,1)S(1)} %all-to-all-done.3.oa0_ref), channel_id=1, source_target_pairs={{0,1},{1,0},{2,3},{3,2},{4,5},{5,4},{6,7},{7,6},{8,9},{9,8},{10,11... | collective-permute-start | bytes 3145736 | tf_op jit(solution)/shard_map/ppermute | solution.py:21
  163.9 21.1 %collective-permute-start.9 = (bf16[4,512,256]{2,1,0:T(8,128)(2,1)}, bf16[4,512,256]{2,1,0:T(8,128)(2,1)}, u32[]{:S(2)}, u32[]{:S(2)}) collective-permute-start(bf16[4,512,256]{2,1,0:T(8,128)(2,1)} %collective-permute-done.7.ob0_ref), channel_id=1, source_target_pairs={{0,1},{1,0},{2,3},{3,2},{4,5},{5,4},{6,7},{7,6},{8,9},{9,8},{10,11... | collective-permute-start | bytes 3145736 | tf_op jit(solution)/shard_map/ppermute | solution.py:21
  170.6 1.2 copy-start.1
  171.8 1.2 copy-start.2
  178.7 6.4 %copy-start.4 = (f32[1024]{0:T(1024)S(1)}, f32[1024]{0:T(1024)}, u32[]{:S(2)}) copy-start(f32[1024]{0:T(1024)} %param.11) | copy-start | bytes 12292
  178.7 6.4 %copy-start.5 = (f32[1024]{0:T(1024)S(1)}, f32[1024]{0:T(1024)}, u32[]{:S(2)}) copy-start(f32[1024]{0:T(1024)} %param.12) | copy-start | bytes 12292

commit v3 on v2

--- a/solution.py
+++ b/solution.py
@@ -12,9 +12,12 @@
 LANES = 128
 
 
-def spread(block, axis):
-    members = lax.axis_size(axis)
-    return lax.all_to_all(jnp.broadcast_to(block, (members, *block.shape)), axis, 0, 0)
+def copies(block, axis):
+    return jnp.broadcast_to(block, (lax.axis_size(axis), *block.shape))
+
+
+def exchanged(blocks, axis):
+    return lax.all_to_all(blocks, axis, 0, 0)
 
 
 def swapped(array, axis):
@@ -38,27 +41,32 @@
     return jnp.concatenate(parts, axis=1)
 
 
-def convolve(where_ref, halo_ref, tok_ref, cw_ref, v0_ref, v1_ref, g0_ref, g1_ref, conv_ref, stats_ref, tok, shifted, cw):
-    par = where_ref[1]
+def prepare(where_ref, halo_ref, tok_ref, cw_ref, tok, cw):
+    deep = tok_ref.shape[1] // 8
+    for at in range(8):
+        here = slice(at * deep, (at + 1) * deep)
+        tok[:HALO, here] = halo_ref[:, columns(where_ref, at // 2, at % 2, deep)]
+        tok[HALO:, here] = tok_ref[:, columns(where_ref, at // 2, at % 2, deep)]
+    for s in range(2):
+        par = where_ref[1] if s == 0 else 1 - where_ref[1]
+        cw[s] = chosen(cw_ref[...], par)
+
+
+def convolve(s, tok, cw, value_of, g0_ref, g1_ref, conv_ref, stats_ref, shifted):
     rows, part = conv_ref.shape
-    taps = cw_ref.shape[0]
-    blocks, deep = v0_ref.shape[0], v0_ref.shape[-1]
+    taps = cw.shape[1]
+    blocks = g0_ref.shape[0]
     order = [(x, m) for x in range(blocks) for m in range(2)]
-    for at, (x, m) in enumerate(order):
-        here = slice(at * deep, (at + 1) * deep)
-        tok[:HALO, here] = halo_ref[:, columns(where_ref, x, m, deep)]
-        tok[HALO:, here] = tok_ref[:, columns(where_ref, x, m, deep)]
-    cw[...] = chosen(cw_ref[...], par)
 
     half = rows // 2
     for q in range(part // PIECE):
         span = slice(q * PIECE, (q + 1) * PIECE)
 
-        def product(*refs):
-            piece = jnp.concatenate([refs[m][x, span, :] for x, m in order], axis=1)
+        def product(of):
+            piece = jnp.concatenate([of(m, x, span) for x, m in order], axis=1)
             return lax.dot_general(tok[...], piece, (((1,), (1,)), ((), ())), preferred_element_type=jnp.float32)
 
-        value, gate = product(v0_ref, v1_ref), product(g0_ref, g1_ref)
+        value, gate = product(value_of), product(lambda m, x, span: (g0_ref, g1_ref)[m][x, span, :])
         glu = (value * jax.nn.sigmoid(gate)).astype(jnp.bfloat16).astype(jnp.float32)
         shifted[0] = glu
         for r in range(1, 8):
@@ -71,7 +79,7 @@
                 for k in range(taps):
                     r, j = k % 8, k // 8
                     begin = HALO - 8 * j + h * half
-                    acc = acc + cw[k : k + 1, at : at + LANES] * shifted[r, begin : begin + half, lanes]
+                    acc = acc + cw[s, k : k + 1, at : at + LANES] * shifted[r, begin : begin + half, lanes]
                 acc = acc.astype(jnp.bfloat16)
                 when = slice(h * half, (h + 1) * half)
                 conv_ref[when, at : at + LANES] = acc
@@ -84,13 +92,22 @@
                     stats_ref[1, when] += acc * acc
 
 
+def first_half(where_ref, halo_ref, tok_ref, cw_ref, ov0_ref, ov1_ref, g0_ref, g1_ref, conv_ref, stats_ref, tok, cw, shifted):
+    prepare(where_ref, halo_ref, tok_ref, cw_ref, tok, cw)
+    convolve(0, tok, cw, lambda m, x, span: (ov0_ref, ov1_ref)[m][x, 1, span, :], g0_ref, g1_ref, conv_ref, stats_ref, shifted)
+
+
+def second_half(where_ref, tok, cw, v0_ref, v1_ref, g0_ref, g1_ref, conv_ref, stats_ref, shifted):
+    convolve(1, tok, cw, lambda m, x, span: (v0_ref, v1_ref)[m][x, span, :], g0_ref, g1_ref, conv_ref, stats_ref, shifted)
+
+
 def finish(
     where_ref, conv_a_ref, conv_b_ref, stats_a_ref, stats_b_ref, gain_ref, bias_ref,
-    oa0_ref, ob0_ref, oa1_ref, ob1_ref, out_ref, normed,
+    ov0_ref, ob0_ref, ov1_ref, ob1_ref, out_ref, normed,
 ):
     side = where_ref[1]
     part = conv_a_ref.shape[1]
-    blocks, deep = oa0_ref.shape[0], oa0_ref.shape[-1]
+    blocks, deep = ob0_ref.shape[0], ob0_ref.shape[-1]
     mean = jnp.sum(stats_a_ref[0] + stats_b_ref[0], axis=1, keepdims=True) / (2 * part)
     meansq = jnp.sum(stats_a_ref[1] + stats_b_ref[1], axis=1, keepdims=True) / (2 * part)
     scale = lax.rsqrt(meansq - mean * mean + EPS)
@@ -104,8 +121,8 @@
             here = slice(s * part + q * PIECE, s * part + (q + 1) * PIECE)
             normed[:, here] = (v / (1.0 + jnp.exp(-v))).astype(jnp.bfloat16)
     for x in range(blocks):
-        for m, (own, other) in enumerate(((oa0_ref, ob0_ref), (oa1_ref, ob1_ref))):
-            right = jnp.concatenate([own[x], other[x]], axis=0)
+        for m, (own, other) in enumerate(((ov0_ref, ob0_ref), (ov1_ref, ob1_ref))):
+            right = jnp.concatenate([own[x, 0], other[x]], axis=0)
             out = jnp.dot(normed[...], right, preferred_element_type=jnp.float32)
             out_ref[:, columns(where_ref, x, m, deep)] = out.astype(jnp.bfloat16)
 
@@ -143,35 +160,34 @@
     near, last, conv_weight, norm_gain, norm_bias = lax.optimization_barrier((near, last, conv_weight, norm_gain, norm_bias))
     v, g, o = near
 
-    ga0 = spread(g, "x")
+    ga0 = exchanged(copies(g, "x"), "x")
     v_other = swapped(v, "side")
     halo = lax.ppermute(last, ("zh", "zl"), [(i, i + 1) for i in range(positions - 1)])
-    oa0 = spread(o, "x")
+    ov0 = exchanged(copies(jnp.stack([o, v]), "x"), "x")
     gb0 = swapped(ga0, "side")
     ga1 = swapped(ga0, "core")
-    va0 = spread(v, "x")
-    ob0 = swapped(oa0, "side")
-    oa1 = swapped(oa0, "core")
-    vb0 = spread(v_other, "x")
-    va1 = swapped(va0, "core")
+    ob0 = swapped(ov0[:, 0], "side")
+    vb0 = exchanged(copies(v_other, "x"), "x")
+    ov1 = swapped(ov0, "core")
     gb1 = swapped(gb0, "core")
     vb1 = swapped(vb0, "core")
     ob1 = swapped(ob0, "core")
-    here, there = (jnp.stack([core, s]).astype(jnp.int32) for s in (side, 1 - side))
+    where = jnp.stack([core, side]).astype(jnp.int32)
     part = channels // 2
-    made = (jax.ShapeDtypeStruct((length, part), jnp.bfloat16), jax.ShapeDtypeStruct((2, length, LANES), jnp.float32))
-    scratch = [
-        pltpu.VMEM((length + HALO, depth), jnp.bfloat16),
-        pltpu.VMEM((8, length + HALO, PIECE), jnp.float32),
-        pltpu.VMEM((conv_weight.shape[0], part), jnp.float32),
-    ]
+    shape = jax.ShapeDtypeStruct
+    made = (shape((length, part), jnp.bfloat16), shape((2, length, LANES), jnp.float32))
+    ready = (shape((length + HALO, depth), jnp.bfloat16), shape((2, conv_weight.shape[0], part), jnp.float32))
+    scratch = [pltpu.VMEM((8, length + HALO, PIECE), jnp.float32)]
     flops = 2 * length * depth * channels
-    conv_a, stats_a = kernel(convolve, made, scratch, flops, 20, here, halo, rows, conv_weight, va0, va1, ga0, ga1)
-    conv_b, stats_b = kernel(convolve, made, scratch, flops, 20, there, halo, rows, conv_weight, vb0, vb1, gb0, gb1)
+    conv_a, stats_a, tok, cw = kernel(
+        first_half, made + ready, scratch, flops, 20,
+        where, halo, rows, conv_weight, ov0, ov1, ga0, ga1,
+    )
+    conv_b, stats_b = kernel(second_half, made, scratch, flops, 20, where, tok, cw, vb0, vb1, gb0, gb1)
     mixed = kernel(
         finish, jax.ShapeDtypeStruct((length, depth), jnp.bfloat16),
         [pltpu.VMEM((length, channels), jnp.bfloat16)], flops, 16,
-        here, conv_a, conv_b, stats_a, stats_b, norm_gain[None], norm_bias[None], oa0, ob0, oa1, ob1,
+        where, conv_a, conv_b, stats_a, stats_b, norm_gain[None], norm_bias[None], ov0, ob0, ov1, ob1,
     )
     return mixed[None]
 

time: 192 us -> 197 us (1.026)
  waiting for transfers between devices: 4.52 us -> 16.7 us
  blocking collectives: 106 us -> 98.2 us
  starting transfers between devices: 57.1 us -> 54 us
  local copies, waits for them, and re-layouts: 4.85 us -> 7.4 us
    ppermute x9 -> x8, waiting for transfers between devices: 0.02 us -> 13.5 us  [swapped(): return lax.ppermute(array, axis, [(0, 1), (1, 0)])]
    all_to_all x2 -> x1, blocking collectives: 28.7 us -> 21.5 us  [exchanged(): return lax.all_to_all(blocks, axis, 0, 0)]
    ppermute x9 -> x8, starting transfers between devices: 46.3 us -> 42.5 us  [swapped(): return lax.ppermute(array, axis, [(0, 1), (1, 0)])]
  transfers between devices with their start and end apart: 12 -> 11, of which waited for: 2 -> 3; matrix products, arithmetic and copies ran while one was open for 1% -> 2% of each run, Pallas kernels for 6% -> 7%
where the time goes in v3:
time: 197 us
  blocking collectives  98.2 us (50%)
  starting transfers between devices  54 us (27%)
  Pallas kernels  19.2 us (10%)
  waiting for transfers between devices  16.7 us (8%)
  local copies, waits for them, and re-layouts  7.4 us (4%)
    all_gather x1, blocking collectives, per_device(): far = lax.all_gather(mine, 'zh', axis=0, tiled=True)  69 us
    ppermute x8, starting transfers between devices, swapped(): return lax.ppermute(array, axis, [(0, 1), (1, 0)])  42.5 us
    all_to_all x1, blocking collectives, exchanged(): return lax.all_to_all(blocks, axis, 0, 0)  21.5 us
    pallas_call x3, Pallas kernels, kernel(): pl.pallas_call(function, out_shape=out_shape, in_specs=[SMEM] + [VMEM] *...  19.2 us
    ppermute x8, waiting for transfers between devices, swapped(): return lax.ppermute(array, axis, [(0, 1), (1, 0)])  13.5 us
    all_to_all x2, starting transfers between devices, exchanged(): return lax.all_to_all(blocks, axis, 0, 0)  8.03 us
    all_gather x1, blocking collectives, per_device(): near = lax.all_gather(far, 'zl', axis=0, tiled=True)  7.68 us
  transfers between devices with their start and end apart: 11, of which 3 were waited for; matrix products, arithmetic and copies ran while one was open for 2% of the time, Pallas kernels for 7%

profile of v3, /device:TPU:33, one launch (start us, length us, event | category | flops | bytes accessed | tf_op | source)
XLA Modules:
  0.0 196.6 jit_solution(792181988351544575)
XLA Ops:
  0.7 69.0 %all_gather.6 = bf16[48,16,256]{2,1,0:T(8,128)(2,1)S(1)} all-gather(bf16[3,16,256]{2,1,0:T(8,128)(2,1)S(1)} %fusion.1), channel_id=1, replica_groups=mesh['pair'=1,'side'=2,'zh'=16,'zl'=2,'x'=4,'core'=2] {'zh'}, dimensions={0}, use_global_device_ids=true | all-gather | bytes 417792 | tf_op jit(solution)/shard_map/all_gather | solution.py:155
  69.8 7.7 %all_gather.7 = bf16[96,16,256]{2,1,0:T(8,128)(2,1)S(1)} all-gather(bf16[48,16,256]{2,1,0:T(8,128)(2,1)S(1)} %all_gather.6), channel_id=1, replica_groups=mesh['pair'=1,'side'=2,'zh'=16,'zl'=2,'x'=4,'core'=2] {'zl'}, dimensions={0}, use_global_device_ids=true | all-gather | bytes 1179648 | tf_op jit(solution)/shard_map/all_gather | solution.py:156
  77.6 1.6 slice_bitcast_fusion.2
  79.4 21.5 %all_to_all.15.ov0_ref = bf16[4,2,512,256]{3,2,1,0:T(8,128)(2,1)S(1)} all-to-all(bf16[4,2,512,256]{3,2,1,0:T(8,128)(2,1)S(1)} %broadcast_in_dim.18), channel_id=1, replica_groups=mesh['pair'=1,'side'=2,'zh'=16,'zl'=2,'x'=4,'core'=2] {'x'}, dimensions={0} | all-to-all | bytes 4194304 | tf_op jit(solution)/shard_map/all_to_all | solution.py:20
  100.9 1.0 broadcast_in_dim.19
  102.0 3.6 %all-to-all-start.1 = ((bf16[4,512,256]{2,1,0:T(8,128)(2,1)}), bf16[4,512,256]{2,1,0:T(8,128)(2,1)S(1)}, u32[]{:S(2)}, u32[]{:S(2)}) async-start(bf16[4,512,256]{2,1,0:T(8,128)(2,1)} %broadcast_in_dim.19), calls=%async_computation.1 | async-start | bytes 2097152 | tf_op jit(solution)/shard_map/all_to_all | solution.py:20
  105.6 12.0 %collective-permute-start.1 = (bf16[4,2,512,256]{3,2,1,0:T(8,128)(2,1)S(1)}, bf16[4,2,512,256]{3,2,1,0:T(8,128)(2,1)}, u32[]{:S(2)}, u32[]{:S(2)}) collective-permute-start(bf16[4,2,512,256]{3,2,1,0:T(8,128)(2,1)S(1)} %all_to_all.15.ov0_ref), channel_id=1, source_target_pairs={{0,1},{1,0},{2,3},{3,2},{4,5},{5,4},{6,7},{7,6},{8,9},{9,8},{10,11... | collective-permute-start | bytes 6291464 | tf_op jit(solution)/shard_map/ppermute | solution.py:24
  117.6 3.8 %collective-permute-start.3 = (bf16[512,256]{1,0:T(8,128)(2,1)S(1)}, bf16[512,256]{1,0:T(8,128)(2,1)}, u32[]{:S(2)}, u32[]{:S(2)}) collective-permute-start(bf16[512,256]{1,0:T(8,128)(2,1)S(1)} %get-tuple-element.27), channel_id=1, source_target_pairs={{0,256},{256,0},{1,257},{257,1},{2,258},{258,2},{3,259},{259,3},{4... | collective-permute-start | bytes 786440 | tf_op jit(solution)/shard_map/ppermute | solution.py:24
  121.4 2.0 collective-permute-start.5
  123.4 1.1 slice_bitcast_fusion
  124.4 3.5 %collective-permute-start.7 = (bf16[4,512,256]{2,1,0:T(8,128)(2,1)}, bf16[4,512,256]{2,1,0:T(8,128)(2,1)}, u32[]{:S(2)}, u32[]{:S(2)}) collective-permute-start(bf16[4,512,256]{2,1,0:T(8,128)(2,1)} %slice_bitcast_fusion), channel_id=1, source_target_pairs={{0,256},{256,0},{1,257},{257,1},{2,258},{258,2},{3,259},{259,3},{4... | collective-permute-start | bytes 3145736 | tf_op jit(solution)/shard_map/ppermute | solution.py:24
  128.1 2.0 %broadcast_in_dim.20 = bf16[4,512,256]{2,1,0:T(8,128)(2,1)} broadcast(bf16[512,256]{1,0:T(8,128)(2,1)} %collective-permute-done.3), dimensions={1,2} | broadcast | bytes 1310720 | tf_op jit(solution)/shard_map/broadcast_in_dim | solution.py:16
  130.1 4.4 %all-to-all-start.2 = ((bf16[4,512,256]{2,1,0:T(8,128)(2,1)}), bf16[4,512,256]{2,1,0:T(8,128)(2,1)}, u32[]{:S(2)}, u32[]{:S(2)}) async-start(bf16[4,512,256]{2,1,0:T(8,128)(2,1)} %broadcast_in_dim.20), calls=%async_computation.2 | async-start | bytes 2097152 | tf_op jit(solution)/shard_map/all_to_all | solution.py:20
  134.6 7.4 %collective-permute-start.2 = (bf16[4,512,256]{2,1,0:T(8,128)(2,1)S(1)}, bf16[4,512,256]{2,1,0:T(8,128)(2,1)}, u32[]{:S(2)}, u32[]{:S(2)}) collective-permute-start(bf16[4,512,256]{2,1,0:T(8,128)(2,1)S(1)} %all-to-all-done.1.g0_ref), channel_id=1, source_target_pairs={{0,1},{1,0},{2,3},{3,2},{4,5},{5,4},{6,7},{7,6},{8,9},{9,8},{10,11... | collective-permute-start | bytes 3145736 | tf_op jit(solution)/shard_map/ppermute | solution.py:24
  142.0 3.5 %collective-permute-start = (bf16[32,2048]{1,0:T(8,128)(2,1)}, bf16[32,2048]{1,0:T(8,128)(2,1)S(1)}, u32[]{:S(2)}, u32[]{:S(2)}) collective-permute-start(bf16[32,2048]{1,0:T(8,128)(2,1)} %slice_bitcast_fusion.2), channel_id=1, source_target_pairs={{0,8},{8,16},{16,24},{24,32},{32,40},{40,48},{48,56},{56,64},{64,7... | collective-permute-start | bytes 393224 | tf_op jit(solution)/shard_map/ppermute | solution.py:165
  145.5 3.1 %collective-permute-done.halo_ref = bf16[32,2048]{1,0:T(8,128)(2,1)S(1)} collective-permute-done((bf16[32,2048]{1,0:T(8,128)(2,1)}, bf16[32,2048]{1,0:T(8,128)(2,1)S(1)}, u32[]{:S(2)}, u32[]{:S(2)}) %collective-permute-start) | collective-permute-done | bytes 131104 | tf_op jit(solution)/shard_map/ppermute | solution.py:165
  148.6 4.2 %collective-permute-start.4 = (bf16[4,512,256]{2,1,0:T(8,128)(2,1)}, bf16[4,512,256]{2,1,0:T(8,128)(2,1)}, u32[]{:S(2)}, u32[]{:S(2)}) collective-permute-start(bf16[4,512,256]{2,1,0:T(8,128)(2,1)} %all-to-all-done.2.v0_ref), channel_id=1, source_target_pairs={{0,1},{1,0},{2,3},{3,2},{4,5},{5,4},{6,7},{7,6},{8,9},{9,8},{10,11... | collective-permute-start | bytes 3145736 | tf_op jit(solution)/shard_map/ppermute | solution.py:24
  152.9 3.7 %collective-permute-start.6 = (bf16[4,512,256]{2,1,0:T(8,128)(2,1)}, bf16[4,512,256]{2,1,0:T(8,128)(2,1)}, u32[]{:S(2)}, u32[]{:S(2)}) collective-permute-start(bf16[4,512,256]{2,1,0:T(8,128)(2,1)} %collective-permute-done.5.g0_ref), channel_id=1, source_target_pairs={{0,1},{1,0},{2,3},{3,2},{4,5},{5,4},{6,7},{7,6},{8,9},{9,8},{10,11... | collective-permute-start | bytes 3145736 | tf_op jit(solution)/shard_map/ppermute | solution.py:24
  156.5 13.3 %collective-permute-done.7.ob0_ref = bf16[4,512,256]{2,1,0:T(8,128)(2,1)} collective-permute-done((bf16[4,512,256]{2,1,0:T(8,128)(2,1)}, bf16[4,512,256]{2,1,0:T(8,128)(2,1)}, u32[]{:S(2)}, u32[]{:S(2)}) %collective-permute-start.7) | collective-permute-done | bytes 1048608 | tf_op jit(solution)/shard_map/ppermute | solution.py:24
  169.9 5.9 %collective-permute-start.8 = (bf16[4,512,256]{2,1,0:T(8,128)(2,1)}, bf16[4,512,256]{2,1,0:T(8,128)(2,1)}, u32[]{:S(2)}, u32[]{:S(2)}) collective-permute-start(bf16[4,512,256]{2,1,0:T(8,128)(2,1)} %collective-permute-done.7.ob0_ref), channel_id=1, source_target_pairs={{0,1},{1,0},{2,3},{3,2},{4,5},{5,4},{6,7},{7,6},{8,9},{9,8},{10,11... | collective-permute-start | bytes 3145736 | tf_op jit(solution)/shard_map/ppermute | solution.py:24
  175.9 1.4 copy-done
  177.3 6.3 %shard_map.73 = (bf16[384,512]{1,0:T(8,128)(2,1)S(1)}, f32[2,384,128]{2,1,0:T(8,128)S(1)}, bf16[416,2048]{1,0:T(8,128)(2,1)S(1)}, f32[2,31,512]{2,1,0:T(8,128)S(1)}) custom-call(s32[2]{0:T(128)S(1)} %pad_add_fusion.where_ref, bf16[32,2048]{1,0:T(8,128)(2,1)S(1)} %collective-permute-done.halo_ref, bf16[384,2048]{1,0:T(8,128)(2,1)S(1)} %bitcast.27, ...), custom_call_target="tpu_custom_call" | custom-call | flops 1610612736 | bytes 8388608 | tf_op jit(solution)/shard_map/pallas_call | solution.py:135
  183.7 6.6 %shard_map.74 = (bf16[384,512]{1,0:T(8,128)(2,1)S(1)}, f32[2,384,128]{2,1,0:T(8,128)S(1)}) custom-call(s32[2]{0:T(128)S(1)} %pad_add_fusion.where_ref, bf16[416,2048]{1,0:T(8,128)(2,1)S(1)} %get-tuple-element.20.tok, f32[2,31,512]{2,1,0:T(8,128)S(1)} %get-tuple-element.21.cw, bf16[4,512,256]{2,1,0:T(8,128)(2,1)} %all-to-all-done.2.v0_ref, ...), custom_call_target="tpu_custom_call" | custom-call | flops 1610612736 | bytes 8388608 | tf_op jit(solution)/shard_map/pallas_call | solution.py:135
  190.3 6.3 %shard_map.75 = bf16[384,2048]{1,0:T(8,128)(2,1)} custom-call(s32[2]{0:T(128)S(1)} %pad_add_fusion.where_ref, bf16[384,512]{1,0:T(8,128)(2,1)S(1)} %get-tuple-element.19.conv_a_ref, bf16[384,512]{1,0:T(8,128)(2,1)S(1)} %get-tuple-element.22.conv_b_ref, f32[2,384,128]{2,1,0:T(8,128)S(1)} %get-tuple-element.23.stats_a_ref, ...), custom_call_target="tpu_custom_call" | custom-call | flops 1610612736 | bytes 8388608 | tf_op jit(solution)/shard_map/pallas_call | solution.py:135
  (22 shorter events, 1.4 us)
Async XLA Ops:
  102.0 19.4 %all-to-all-start.1 = ((bf16[4,512,256]{2,1,0:T(8,128)(2,1)}), bf16[4,512,256]{2,1,0:T(8,128)(2,1)S(1)}, u32[]{:S(2)}, u32[]{:S(2)}) async-start(bf16[4,512,256]{2,1,0:T(8,128)(2,1)} %broadcast_in_dim.19), calls=%async_computation.1 | async-start | bytes 2097152 | tf_op jit(solution)/shard_map/all_to_all | solution.py:20
  105.6 70.3 %collective-permute-start.1 = (bf16[4,2,512,256]{3,2,1,0:T(8,128)(2,1)S(1)}, bf16[4,2,512,256]{3,2,1,0:T(8,128)(2,1)}, u32[]{:S(2)}, u32[]{:S(2)}) collective-permute-start(bf16[4,2,512,256]{3,2,1,0:T(8,128)(2,1)S(1)} %all_to_all.15.ov0_ref), channel_id=1, source_target_pairs={{0,1},{1,0},{2,3},{3,2},{4,5},{5,4},{6,7},{7,6},{8,9},{9,8},{10,11... | collective-permute-start | bytes 6291464 | tf_op jit(solution)/shard_map/ppermute | solution.py:24
  117.6 10.5 %collective-permute-start.3 = (bf16[512,256]{1,0:T(8,128)(2,1)S(1)}, bf16[512,256]{1,0:T(8,128)(2,1)}, u32[]{:S(2)}, u32[]{:S(2)}) collective-permute-start(bf16[512,256]{1,0:T(8,128)(2,1)S(1)} %get-tuple-element.27), channel_id=1, source_target_pairs={{0,256},{256,0},{1,257},{257,1},{2,258},{258,2},{3,259},{259,3},{4... | collective-permute-start | bytes 786440 | tf_op jit(solution)/shard_map/ppermute | solution.py:24
  121.4 31.4 %collective-permute-start.5 = (bf16[4,512,256]{2,1,0:T(8,128)(2,1)S(1)}, bf16[4,512,256]{2,1,0:T(8,128)(2,1)}, u32[]{:S(2)}, u32[]{:S(2)}) collective-permute-start(bf16[4,512,256]{2,1,0:T(8,128)(2,1)S(1)} %all-to-all-done.1.g0_ref), channel_id=1, source_target_pairs={{0,256},{256,0},{1,257},{257,1},{2,258},{258,2},{3,259},{259,3},{4... | collective-permute-start | bytes 3145736 | tf_op jit(solution)/shard_map/ppermute | solution.py:24
  124.4 51.5 %copy-start.1 = (bf16[31,1024]{1,0:T(8,128)(2,1)S(1)}, bf16[31,1024]{1,0:T(8,128)(2,1)}, u32[]{:S(2)}) copy-start(bf16[31,1024]{1,0:T(8,128)(2,1)} %cw_ref) | copy-start | bytes 190468
  124.4 45.4 %collective-permute-start.7 = (bf16[4,512,256]{2,1,0:T(8,128)(2,1)}, bf16[4,512,256]{2,1,0:T(8,128)(2,1)}, u32[]{:S(2)}, u32[]{:S(2)}) collective-permute-start(bf16[4,512,256]{2,1,0:T(8,128)(2,1)} %slice_bitcast_fusion), channel_id=1, source_target_pairs={{0,256},{256,0},{1,257},{257,1},{2,258},{258,2},{3,259},{259,3},{4... | collective-permute-start | bytes 3145736 | tf_op jit(solution)/shard_map/ppermute | solution.py:24
  130.1 18.5 %all-to-all-start.2 = ((bf16[4,512,256]{2,1,0:T(8,128)(2,1)}), bf16[4,512,256]{2,1,0:T(8,128)(2,1)}, u32[]{:S(2)}, u32[]{:S(2)}) async-start(bf16[4,512,256]{2,1,0:T(8,128)(2,1)} %broadcast_in_dim.20), calls=%async_computation.2 | async-start | bytes 2097152 | tf_op jit(solution)/shard_map/all_to_all | solution.py:20
  134.6 41.3 %collective-permute-start.2 = (bf16[4,512,256]{2,1,0:T(8,128)(2,1)S(1)}, bf16[4,512,256]{2,1,0:T(8,128)(2,1)}, u32[]{:S(2)}, u32[]{:S(2)}) collective-permute-start(bf16[4,512,256]{2,1,0:T(8,128)(2,1)S(1)} %all-to-all-done.1.g0_ref), channel_id=1, source_target_pairs={{0,1},{1,0},{2,3},{3,2},{4,5},{5,4},{6,7},{7,6},{8,9},{9,8},{10,11... | collective-permute-start | bytes 3145736 | tf_op jit(solution)/shard_map/ppermute | solution.py:24
  142.0 6.7 %collective-permute-start = (bf16[32,2048]{1,0:T(8,128)(2,1)}, bf16[32,2048]{1,0:T(8,128)(2,1)S(1)}, u32[]{:S(2)}, u32[]{:S(2)}) collective-permute-start(bf16[32,2048]{1,0:T(8,128)(2,1)} %slice_bitcast_fusion.2), channel_id=1, source_target_pairs={{0,8},{8,16},{16,24},{24,32},{32,40},{40,48},{48,56},{56,64},{64,7... | collective-permute-start | bytes 393224 | tf_op jit(solution)/shard_map/ppermute | solution.py:165
  148.6 35.0 %collective-permute-start.4 = (bf16[4,512,256]{2,1,0:T(8,128)(2,1)}, bf16[4,512,256]{2,1,0:T(8,128)(2,1)}, u32[]{:S(2)}, u32[]{:S(2)}) collective-permute-start(bf16[4,512,256]{2,1,0:T(8,128)(2,1)} %all-to-all-done.2.v0_ref), channel_id=1, source_target_pairs={{0,1},{1,0},{2,3},{3,2},{4,5},{5,4},{6,7},{7,6},{8,9},{9,8},{10,11... | collective-permute-start | bytes 3145736 | tf_op jit(solution)/shard_map/ppermute | solution.py:24
  152.9 30.8 %collective-permute-start.6 = (bf16[4,512,256]{2,1,0:T(8,128)(2,1)}, bf16[4,512,256]{2,1,0:T(8,128)(2,1)}, u32[]{:S(2)}, u32[]{:S(2)}) collective-permute-start(bf16[4,512,256]{2,1,0:T(8,128)(2,1)} %collective-permute-done.5.g0_ref), channel_id=1, source_target_pairs={{0,1},{1,0},{2,3},{3,2},{4,5},{5,4},{6,7},{7,6},{8,9},{9,8},{10,11... | collective-permute-start | bytes 3145736 | tf_op jit(solution)/shard_map/ppermute | solution.py:24
  169.9 20.4 %collective-permute-start.8 = (bf16[4,512,256]{2,1,0:T(8,128)(2,1)}, bf16[4,512,256]{2,1,0:T(8,128)(2,1)}, u32[]{:S(2)}, u32[]{:S(2)}) collective-permute-start(bf16[4,512,256]{2,1,0:T(8,128)(2,1)} %collective-permute-done.7.ob0_ref), channel_id=1, source_target_pairs={{0,1},{1,0},{2,3},{3,2},{4,5},{5,4},{6,7},{7,6},{8,9},{9,8},{10,11... | collective-permute-start | bytes 3145736 | tf_op jit(solution)/shard_map/ppermute | solution.py:24
  175.9 1.4 copy-start
  183.7 6.6 %copy-start.2 = (f32[1024]{0:T(1024)S(1)}, f32[1024]{0:T(1024)}, u32[]{:S(2)}) copy-start(f32[1024]{0:T(1024)} %param.11) | copy-start | bytes 12292
  183.7 6.6 %copy-start.3 = (f32[1024]{0:T(1024)S(1)}, f32[1024]{0:T(1024)}, u32[]{:S(2)}) copy-start(f32[1024]{0:T(1024)} %param.12) | copy-start | bytes 12292
